TPU v7x, 128 devices: a whole 4x4x4 slice. The times are simulated.
128 devices in a mesh: sp: 16 (over z, x), dp: 8 (over y, core).
Axes of the slice: x: 4, y: 4, z: 4, core: 2. Of those that a mesh axis runs over, the one named last changes fastest.
Arguments:
- hidden_in: bfloat16 [8, 2048, 2048], P('dp', 'sp'), may hold values from -6 to 6
- mix_cotangent: bfloat16 [8, 2048, 4096], P('dp', 'sp'), may hold values from -0.119628906 to 0.119628906
- query_weight: bfloat16 [2048, 4096], P('dp', 'sp'), may hold values from -0.125 to 0.125
- key_weight: bfloat16 [2048, 4096], P('dp', 'sp'), may hold values from -0.125 to 0.125
- value_weight: bfloat16 [2048, 4096], P('dp', 'sp'), may hold values from -0.125 to 0.125
- decay_log: float32 [16], P('sp'), may hold values from -0.034 to -0.000146484375, as said below
Outputs:
- grad_hidden: bfloat16 [8, 2048, 2048], P('dp', 'sp')
- grad_query: float32 [2048, 4096], P('dp', 'sp')
- grad_key: float32 [2048, 4096], P('dp', 'sp')
- grad_value: float32 [2048, 4096], P('dp', 'sp')
Inputs may be any that keep to these rules, and one draw needn't show every extreme that they name: Each head's decay_log is negative.
All inputs are finite; a program needn't handle non-finite values.
Results may differ from a plain program's by a relative error of at most 0.015.
Values may be sent and summed in bfloat16 or wider, within the bound.
A program may use at most 64 MiB of HBM per device.

v0:
```python
import functools

import jax
import jax.numpy as jnp
from jax import lax
from jax.experimental import pallas as pl
from jax.experimental.pallas import tpu as pltpu
from jax.sharding import PartitionSpec as P

BLOCK = 128
SUBS = 2
F32 = jnp.float32
BF16 = jnp.bfloat16
MESH = pl.DeviceIdType.MESH
NT = (((1,), (1,)), ((), ()))
TN = (((0,), (0,)), ((), ()))
VMEM_LIMIT = 52 * 1024 * 1024


def dot(a, b, dims=(((1,), (0,)), ((), ()))):
    return lax.dot_general(a, b, dims, preferred_element_type=F32)


def remote(src, dst, send, recv, where):
    return pltpu.make_async_remote_copy(
        src_ref=src, dst_ref=dst, send_sem=send, recv_sem=recv, device_id=where, device_id_type=MESH
    )


def greet(targets):
    barrier = pltpu.get_barrier_semaphore()
    for where in targets:
        pl.semaphore_signal(barrier, inc=1, device_id=where, device_id_type=MESH)
    pl.semaphore_wait(barrier, len(targets))


def gather_phase(
    n, m, project, h_in, c_in, wq, wk, wv, h_all, c_all, w_all,
    h_recv, h_line, h_side, c_send, c_recv, w_far, w_near, w_recv,
):
    s = lax.axis_index("sp")
    d = lax.axis_index("dp")
    z, x = s // 2, s % 2
    y, core = d // 2, d % 2
    nz, ny = n // 2, m // 2
    rows = h_in.shape[0]
    sub_rows = rows // SUBS
    depth, columns = wq.shape
    side = s + 1 - 2 * x
    mate = d + 1 - 2 * core

    def far(o):
        return ((y + o) % ny) * 2 + core

    greet(
        [{"sp": (s + k) % n} for k in range(1, n)]
        + [{"dp": mate}]
        + [{"dp": far(o)} for o in range(1, ny)]
    )

    def h_copy(src_z, src_x, sub, dest, send, own=False):
        block = src_z * 2 + src_x
        place = pl.ds(pl.multiple_of(block * rows + sub * sub_rows, sub_rows), sub_rows)
        src = h_in.at[pl.ds(sub * sub_rows, sub_rows)] if own else h_all.at[place]
        return remote(src, h_all.at[place], send, h_recv.at[block, sub], {"sp": dest})

    def w_copy(src_d, j, dest, send, own=False):
        place = w_all.at[
            pl.ds(pl.multiple_of(src_d * depth, depth), depth), pl.ds(j * columns, columns)
        ]
        return remote((wq, wk, wv)[j] if own else place, place, send, w_recv.at[src_d, j], {"dp": dest})

    def c_copy(k):
        to = (s + k) % n
        return remote(
            c_in.at[:, pl.ds(pl.multiple_of(to * columns, columns), columns)],
            c_all.at[pl.ds(pl.multiple_of(s * rows, rows), rows)],
            c_send.at[k - 1],
            c_recv.at[k - 1],
            {"sp": to},
        )

    def line(k, sub, up, own):
        source = (z - k) if up else (z + k)
        dest = (s + 2) if up else (s - 2)
        return h_copy(source, x, sub, dest, h_line.at[k, sub, int(up)], own)

    def goes(k, up):
        if up:
            return jnp.logical_and(z - k >= 0, z + 1 < nz)
        return jnp.logical_and(z + k < nz, z >= 1)

    def arrives(k, up):
        return (z - k >= 0) if up else (z + k < nz)

    for sub in range(SUBS):
        for up in (True, False):

            @pl.when(goes(0, up))
            def _():
                line(0, sub, up, True).start()

        h_copy(z, x, sub, side, h_side.at[0, sub, 0], True).start()
    for j in range(3):
        for o in range(1, ny):
            w_copy(d, j, far(o), w_far.at[o, j], True).start()
        w_copy(d, j, mate, w_near.at[0, j], True).start()

    h_all[pl.ds(pl.multiple_of(s * rows, rows), rows), :] = h_in[...]
    c_all[pl.ds(pl.multiple_of(s * rows, rows), rows), :] = c_in[
        :, pl.ds(pl.multiple_of(s * columns, columns), columns)
    ]
    for j, w in enumerate((wq, wk, wv)):
        w_all[pl.ds(pl.multiple_of(d * depth, depth), depth), j * columns : (j + 1) * columns] = w[...]

    def pass_weights(j):
        for o in range(1, ny):
            w_copy(far(o), j, mate, w_near.at[o, j]).wait_recv()
            w_copy(far(o), j, mate, w_near.at[o, j]).start()

    def send_cotangent():
        for hop in range(1, n):
            c_copy(hop).start()

    passed = 0
    for k in range(1, nz):
        for sub in range(SUBS):
            for up in (True, False):

                @pl.when(arrives(k, up))
                def _():
                    source = (z - k) if up else (z + k)
                    h_copy(source, x, sub, side, h_side.at[k, sub, int(up)]).wait_recv()
                    h_copy(source, x, sub, side, h_side.at[k, sub, int(up)]).start()

                @pl.when(goes(k, up))
                def _():
                    line(k, sub, up, False).start()

    send_cotangent()
    for j in range(passed, 3):
        pass_weights(j)

    for j in range(3):
        w_copy(mate, j, mate, w_near.at[0, j]).wait_recv()
        for o in range(1, ny):
            other = far(o) + 1 - 2 * core
            w_copy(other, j, mate, w_near.at[o, j]).wait_recv()

    @pl.loop(0, nz)
    def _(zz):
        project(zz * 2 + x)

    turn = 1 - 2 * (z // ((nz + 1) // 2))

    @pl.loop(0, nz)
    def _(k):
        zz = (z + turn * k + nz) % nz
        for sub in range(SUBS):
            h_copy(zz, 1 - x, sub, side, h_side.at[0, sub, 0]).wait_recv()
        project(zz * 2 + 1 - x)

    for k in range(1, n):
        c_copy(k).wait_recv()
    def drain():
        for k in range(1, n):
            c_copy(k).wait_send()
        for j in range(3):
            for o in range(ny):
                w_copy(d, j, mate, w_near.at[o, j]).wait_send()
                if o:
                    w_copy(d, j, far(o), w_far.at[o, j]).wait_send()
        for sub in range(SUBS):
            h_copy(z, x, sub, side, h_side.at[0, sub, 0]).wait_send()
            for up in (True, False):
                for k in range(nz):

                    @pl.when(goes(k, up))
                    def _():
                        line(k, sub, up, False).wait_send()

                    if k:

                        @pl.when(arrives(k, up))
                        def _():
                            h_copy(z, x, sub, side, h_side.at[k, sub, int(up)]).wait_send()

    return drain


def project_block(h_all, w_all, p_all, rows, columns, scale, block):
    at = pl.ds(pl.multiple_of(block * rows, rows), rows)
    for j in range(3):
        value = dot(h_all[at, :], w_all[:, j * columns : (j + 1) * columns]).astype(BF16)
        if j == 1:
            value = (value.astype(F32) * scale).astype(BF16)
        p_all[at, j * columns : (j + 1) * columns] = value


def mixer_phase(heads, rate, c_all, p_all, g_all, state, back):
    length, columns = c_all.shape
    dim = columns // heads
    blocks = length // BLOCK
    scale = dim ** (-0.5)
    row = lax.broadcasted_iota(jnp.int32, (BLOCK, BLOCK), 0).astype(F32)
    col = lax.broadcasted_iota(jnp.int32, (BLOCK, BLOCK), 1).astype(F32)
    place = lax.broadcasted_iota(jnp.int32, (BLOCK, dim), 0).astype(F32)
    spread = row - col
    state[...] = jnp.zeros_like(state)
    back[...] = jnp.zeros_like(back)

    @pl.loop(0, blocks)
    def _(i):
        for h in range(heads):
            g = rate[h]
            inner = jnp.where(spread >= 0, jnp.exp(g * jnp.maximum(spread, 0.0)), 0.0)
            inner_t = jnp.where(spread <= 0, jnp.exp(g * jnp.maximum(-spread, 0.0)), 0.0)
            query_decay = jnp.exp(g * (place + 1.0))
            key_decay = jnp.exp(g * (BLOCK - 1.0 - place))
            block_decay = jnp.exp(jnp.full((1, dim), g * BLOCK, F32))
            parts = [slice(j * columns + h * dim, j * columns + (h + 1) * dim) for j in range(3)]

            at = pl.ds(pl.multiple_of(i * BLOCK, BLOCK), BLOCK)
            k, v = p_all[at, parts[1]], p_all[at, parts[2]]
            c = c_all[at, parts[0]]
            mixed = (dot(c, v, NT) * inner).astype(BF16)
            held = state[h]
            grad_q = dot(mixed, k) + dot(c, held.astype(BF16), NT) * query_decay
            weighted = (k.astype(F32) * key_decay).astype(BF16)
            state[h] = held * block_decay + dot(weighted, v, TN)
            g_all[at, parts[0]] = grad_q.astype(BF16)

            at = pl.ds(pl.multiple_of((blocks - 1 - i) * BLOCK, BLOCK), BLOCK)
            q, k, v = (p_all[at, part] for part in parts)
            c = c_all[at, parts[0]]
            mixed_t = (dot(v, c, NT) * inner_t).astype(BF16)
            scores_t = (dot(k, q, NT) * inner_t).astype(BF16)
            held = back[h]
            held_bf = held.astype(BF16)
            grad_v = dot(scores_t, c) + dot(k, held_bf) * key_decay
            grad_k = (dot(mixed_t, q) + dot(v, held_bf, NT) * key_decay) * scale
            weighted = (q.astype(F32) * query_decay).astype(BF16)
            back[h] = held * block_decay + dot(weighted, c, TN)
            g_all[at, parts[1]] = grad_k.astype(BF16)
            g_all[at, parts[2]] = grad_v.astype(BF16)


def scatter_phase(
    n, m, h_all, w_all, g_all, dh, dq, dk, dv,
    part, ring, turned, near_out, near_in, far_out, far_in,
    r_send, r_recv, n_send, n_recv, f_send, f_recv,
):
    s = lax.axis_index("sp")
    d = lax.axis_index("dp")
    z, x = s // 2, s % 2
    y, core = d // 2, d % 2
    nz, ny = n // 2, m // 2
    rows, width = dh.shape
    depth, columns = dq.shape
    half = rows // 2
    sub_rows = half // SUBS
    mate = d + 1 - 2 * core
    me = x * (n - 1 - z) + (1 - x) * z

    def at_ring(p):
        p = (p + 2 * n) % n
        hi = p // nz
        return (hi * (n - 1 - p) + (1 - hi) * p) * 2 + hi

    def far(o):
        return ((y + o) % ny) * 2 + core

    right, left = at_ring(me + 1), at_ring(me - 1)

    def own(offset):
        return pl.multiple_of(at_ring(me + offset) * rows, rows)

    ready = set()

    def compute(*offsets):
        todo = []
        for offset in offsets:
            if offset % n not in ready:
                ready.add(offset % n)
                todo.append(own(offset))
        if not todo:
            return
        chunk = width // 4

        @pl.loop(0, 4)
        def _(i):
            at = pl.ds(pl.multiple_of(i * chunk, chunk), chunk)
            lhs = jnp.concatenate([g_all[pl.ds(base, rows), :] for base in todo], axis=0)
            value = dot(lhs, w_all[at, :], NT).astype(BF16)
            for spot, base in enumerate(todo):
                part[pl.ds(base, rows), at] = value[spot * rows : (spot + 1) * rows]

    def r_copy(step, way, sub):
        lane = (slice(0, half), slice(half, rows))[way].start + sub * sub_rows
        if step == 0:
            base = own(-1 if way == 0 else 1)
            src = part.at[pl.ds(pl.multiple_of(base + lane, sub_rows), sub_rows)]
        else:
            src = ring.at[step - 1, way, sub]
        return remote(
            src,
            ring.at[step, way, sub],
            r_send.at[step, way, sub],
            r_recv.at[step, way, sub],
            {"sp": right if way == 0 else left},
        )

    def process(step):
        for sub in range(SUBS):
            for way in range(2):
                base = own(-(step + 2) if way == 0 else step + 2)
                lane = way * half + sub * sub_rows
                r_copy(step, way, sub).wait_recv()
                mine = part[pl.ds(pl.multiple_of(base + lane, sub_rows), sub_rows), :]
                total = (ring[step, way, sub].astype(F32) + mine.astype(F32)).astype(BF16)
                if step < n - 2:
                    ring[step, way, sub] = total
                    r_copy(step + 1, way, sub).start()
                else:
                    dh[lane : lane + sub_rows, :] = total

    def turn(device):
        turned[...] = h_all[:, pl.ds(pl.multiple_of(device * depth, depth), depth)].T

    def weight_part(j):
        return dot(turned[...], g_all[:, pl.ds(pl.multiple_of(j * columns, columns), columns)])

    def n_copy(o):
        return remote(near_out.at[o], near_in.at[o], n_send.at[o], n_recv.at[o], {"dp": mate})

    def f_copy(o, j):
        return remote(
            far_out.at[o - 1, j], far_in.at[o - 1, j], f_send.at[o - 1, j], f_recv.at[o - 1, j], {"dp": far(o)}
        )

    def near(o):
        turn(far(o) + 1 - 2 * core)

        @pl.loop(0, 3)
        def _(j):
            near_out[o, j] = weight_part(j).astype(BF16)

        n_copy(o).start()

    def chip_sum(o):
        turn(far(o))
        n_copy(o).wait_recv()
        if o:
            for j in range(3):
                far_out[o - 1, j] = (weight_part(j) + near_in[o, j].astype(F32)).astype(BF16)
                f_copy(o, j).start()
        else:
            for j, out in enumerate((dq, dk, dv)):
                out[...] = weight_part(j) + near_in[o, j].astype(F32)

    tasks = []
    for o in range(1, ny):
        tasks += [functools.partial(near, o), functools.partial(chip_sum, o)]
    tasks += [functools.partial(near, 0), functools.partial(chip_sum, 0)]

    compute(-1, 1)
    for sub in range(SUBS):
        for way in range(2):
            r_copy(0, way, sub).start()
    for step in range(n - 1):
        early = step % 2 == 0
        if early and tasks:
            tasks.pop(0)()
        compute(-(step + 2), step + 2)
        process(step)
        if not early and tasks:
            tasks.pop(0)()
        if step == 0 and tasks:
            tasks.pop(0)()
        if step + 3 == n // 2:
            compute(n // 2, 0)
    while tasks:
        tasks.pop(0)()
    for j, out in enumerate((dq, dk, dv)):
        total = out[...]
        for o in range(1, ny):
            f_copy(o, j).wait_recv()
            total = total + far_in[o - 1, j].astype(F32)
        out[...] = total * (1.0 / m)
    for step in range(n - 1):
        for sub in range(SUBS):
            for way in range(2):
                r_copy(step, way, sub).wait_send()
    for o in range(ny):
        n_copy(o).wait_send()
        if o:
            for j in range(3):
                f_copy(o, j).wait_send()


def whole_kernel(n, m, heads, rate, h_in, c_in, wq, wk, wv, dh, dq, dk, dv, *scratch):
    h_all, c_all, w_all, p_all, g_all, state, back = scratch[:7]
    gather_sems, rest = scratch[7:15], scratch[15:]
    columns = wq.shape[1]
    project = functools.partial(
        project_block, h_all, w_all, p_all, h_in.shape[0], columns, (columns // heads) ** (-0.5)
    )
    drain = gather_phase(
        n, m, project, h_in, c_in, wq, wk, wv, h_all, c_all, w_all, *gather_sems
    )
    mixer_phase(heads, rate, c_all, p_all, g_all, state, back)
    scatter_phase(n, m, h_all, w_all, g_all, dh, dq, dk, dv, *rest)
    drain()


def whole(n, m, rate, h, c, wq, wk, wv):
    rows, width = h.shape
    depth, columns = wq.shape
    heads = rate.shape[0]
    dim = columns // heads
    length = rows * n
    ny = m // 2
    vmem = pl.BlockSpec(memory_space=pltpu.VMEM)
    dma = pltpu.SemaphoreType.DMA
    sub_rows = rows // 2 // SUBS
    return pl.pallas_call(
        functools.partial(whole_kernel, n, m, heads),
        out_shape=(pltpu.VMEM((rows, width), BF16),)
        + (pltpu.VMEM((depth, columns), F32),) * 3,
        in_specs=[pl.BlockSpec(memory_space=pltpu.SMEM)] + [vmem] * 5,
        out_specs=(vmem,) * 4,
        scratch_shapes=[
            pltpu.VMEM((length, width), BF16),
            pltpu.VMEM((length, columns), BF16),
            pltpu.VMEM((depth * m, 3 * columns), BF16),
            pltpu.VMEM((length, 3 * columns), BF16),
            pltpu.VMEM((length, 3 * columns), BF16),
            pltpu.VMEM((heads, dim, dim), F32),
            pltpu.VMEM((heads, dim, dim), F32),
            dma((n, SUBS)),
            dma((n // 2, SUBS, 2)),
            dma((n // 2, SUBS, 2)),
            dma((n - 1,)),
            dma((n - 1,)),
            dma((ny, 3)),
            dma((ny, 3)),
            dma((m, 3)),
            pltpu.VMEM((length, width), BF16),
            pltpu.VMEM((n - 1, 2, SUBS, sub_rows, width), BF16),
            pltpu.VMEM((depth, length), BF16),
            pltpu.VMEM((ny, 3, depth, columns), BF16),
            pltpu.VMEM((ny, 3, depth, columns), BF16),
            pltpu.VMEM((ny - 1, 3, depth, columns), BF16),
            pltpu.VMEM((ny - 1, 3, depth, columns), BF16),
            dma((n - 1, 2, SUBS)),
            dma((n - 1, 2, SUBS)),
            dma((ny,)),
            dma((ny,)),
            dma((ny - 1, 3)),
            dma((ny - 1, 3)),
        ],
        compiler_params=pltpu.CompilerParams(
            collective_id=0, has_side_effects=True, vmem_limit_bytes=VMEM_LIMIT
        ),
        name="whole",
    )(rate, h, c, wq, wk, wv)


def finish_kernel(count, *refs):
    ins, outs, sems = refs[:count], refs[count : 2 * count], refs[2 * count]
    moves = [pltpu.make_async_copy(ins[i], outs[i], sems.at[i]) for i in range(count)]
    for move in moves:
        move.start()
    for move in moves:
        move.wait()


def finish(*arrays):
    count = len(arrays)
    return pl.pallas_call(
        functools.partial(finish_kernel, count),
        out_shape=tuple(jax.ShapeDtypeStruct(a.shape, a.dtype) for a in arrays),
        in_specs=[pl.BlockSpec(memory_space=pltpu.VMEM)] * count,
        out_specs=(pl.BlockSpec(memory_space=pl.ANY),) * count,
        scratch_shapes=[pltpu.SemaphoreType.DMA((count,))],
        compiler_params=pltpu.CompilerParams(vmem_limit_bytes=4 * 1024 * 1024),
        name="finish",
    )(*arrays)


def body(n, m, hidden_in, mix_cotangent, query_weight, key_weight, value_weight, decay_log):
    dh, dq, dk, dv = finish(
        *whole(
            n, m, decay_log, hidden_in[0], mix_cotangent[0], query_weight, key_weight, value_weight
        )
    )
    return dh[None], dq, dk, dv


def solution(mesh):
    placed = (
        P("dp", "sp", None),
        P("dp", "sp", None),
        P("dp", "sp"),
        P("dp", "sp"),
        P("dp", "sp"),
        P("sp"),
    )
    return jax.shard_map(
        functools.partial(body, mesh.shape["sp"], mesh.shape["dp"]),
        mesh=mesh,
        in_specs=placed,
        out_specs=(P("dp", "sp", None), P("dp", "sp"), P("dp", "sp"), P("dp", "sp")),
        check_vma=False,
    )
```

profile of v0, /device:TPU:1, one launch (start us, length us, event | category | flops | bytes accessed | tf_op | source)
XLA Modules:
  0.0 430.6 jit_solution(17807793818731395759)
XLA Ops:
  1.3 0.0 copy-start
  1.3 0.9 copy-done
  2.2 0.0 copy-start.1
  2.2 0.9 copy-done.1
  3.1 0.0 copy-start.2
  3.1 0.9 copy-done.2
  4.0 425.3 %whole.1 = (bf16[128,2048]{1,0:T(8,128)(2,1)S(1)}, f32[256,256]{1,0:T(8,128)S(1)}, f32[256,256]{1,0:T(8,128)S(1)}, f32[256,256]{1,0:T(8,128)S(1)}) custom-call(f32[1]{0:T(128)S(6)} %copy.10.rate, bf16[128,2048]{1,0:T(8,128)(2,1)} %bitcast.4, bf16[128,4096]{1,0:T(8,128)(2,1)} %bitcast.3, bf16[256,256]{1,0:T(8,128)(2,1)S(1)} %copy-done, ...), custom_call_target="tpu_custom_call" | custom-call | tf_op jit(solution)/shard_map/whole/pallas_call | solution.py:426
  429.3 1.1 finish.1
Async XLA Ops:
  1.3 0.9 copy-start
  2.2 0.9 copy-start.1
  3.1 0.9 copy-start.2
where the time goes:
time: 431 us
  Pallas kernels  426 us (99%)
    pallas_call x1, Pallas kernels, whole(): pl.pallas_call(functools.partial(whole_kernel, n, m, heads), out_shape=(p...  425 us

commit v1 on v0

v1 whole, which is shorter than its diff:
```python
import functools

import jax
import jax.numpy as jnp
from jax import lax
from jax.experimental import pallas as pl
from jax.experimental.pallas import tpu as pltpu
from jax.sharding import PartitionSpec as P

BLOCK = 128
SIDE = 4
FIRST = 640
F32 = jnp.float32
BF16 = jnp.bfloat16
MESH = pl.DeviceIdType.MESH
NN = (((1,), (0,)), ((), ()))
NT = (((1,), (1,)), ((), ()))
TN = (((0,), (0,)), ((), ()))
VMEM_LIMIT = 60 * 1024 * 1024
SEMS = 160


def dot(a, b, dims=NN):
    return lax.dot_general(a, b, dims, preferred_element_type=F32)


def span(start, size, step):
    return pl.ds(pl.multiple_of(start, step), size)


class Net:
    def __init__(self, send, recv, somewhere):
        self.send, self.recv, self.somewhere = send, recv, somewhere
        self.names, self.starts, self.pending = {}, 0, []

    def index(self, name, width=1):
        if name not in self.names:
            self.names[name] = sum(w for _, w in self.names.values()), width
        return self.names[name][0]

    def start(self, name, src, dst, where, offset=0, width=1, when=None):
        slot = self.index(name, width) + offset
        lane = self.starts
        self.starts += 1

        def make():
            return pltpu.make_async_remote_copy(
                src_ref=src, dst_ref=dst, send_sem=self.send.at[lane], recv_sem=self.recv.at[slot],
                device_id=where, device_id_type=MESH,
            )

        if when is None:
            make().start()
        else:
            pl.when(when)(lambda: make().start())
        self.pending.append((when, make))

    def wait(self, name, dst, offset=0, width=1, when=None):
        slot = self.index(name, width) + offset

        def run():
            pltpu.make_async_remote_copy(
                src_ref=dst, dst_ref=dst, send_sem=self.send.at[0], recv_sem=self.recv.at[slot],
                device_id=self.somewhere, device_id_type=MESH,
            ).wait_recv()

        if when is None:
            run()
        else:
            pl.when(when)(run)

    def drain(self):
        for when, make in self.pending:
            if when is None:
                make().wait_send()
            else:
                pl.when(when)(lambda make=make: make().wait_send())


def whole_kernel(
    rate, h_in, c_in, wq, wk, wv, dh, dq, dk, dv,
    h_all, c_all, w_all, p_all, g_all, state, back, rates, inner, inner_t, decays,
    pout, pin, psum, ra1, ra2, ra3, rb0, rb1, rb2, dbuf,
    ysend, yone, ykeep, yhome, yr1, yr2, yout, yend, send, recv,
):
    s = lax.axis_index("sp")
    d = lax.axis_index("dp")
    z, x = s // SIDE, s % SIDE
    y, c = d // 2, d % 2
    u = x // 2
    xl = x - 2 * u
    own = c == u
    away = c != u
    rows, width = h_in.shape
    depth, columns = wq.shape
    half = width // 2
    four = rows * SIDE
    two = rows * 2
    blocks = SIDE * SIDE
    scale = columns ** (-0.5)

    def at(zz=None, xx=None, yy=None, cc=None):
        zz, xx = z if zz is None else zz, x if xx is None else xx
        yy, cc = y if yy is None else yy, c if cc is None else cc
        return {"sp": zz * SIDE + xx, "dp": yy * 2 + cc}

    def turned(v, by):
        return (v + by + SIDE) % SIDE

    mate = at(cc=1 - c)
    pair = at(xx=x + 1 - 2 * xl)
    zs = {1: at(zz=turned(z, 1)), -1: at(zz=turned(z, -1))}
    ys = {1: at(yy=turned(y, 1)), -1: at(yy=turned(y, -1))}
    cross = 3 - x
    net = Net(send, recv, mate)

    barrier = pltpu.get_barrier_semaphore()
    peers = [mate, ys[1], ys[-1]]
    for k in range(1, blocks):
        other = (s + k) % blocks
        peers += [{"sp": other, "dp": d}, {"sp": other, "dp": y * 2 + 1 - c}]
    for where in peers:
        pl.semaphore_signal(barrier, inc=1, device_id=where, device_id_type=MESH)
    rates[0] = jnp.full(rates.shape[1:], rate[0], F32)
    pl.semaphore_wait(barrier, len(peers))

    def slot(r, col, b):
        return turned(z, r) * SIDE + 2 * (xl if col == 0 else 1 - xl) + b

    def h_ref(place, part, which):
        base = which * half
        lo, size = {"f": (0, half), "a": (0, FIRST), "b": (FIRST, half - FIRST)}[part]
        return h_all.at[span(place * rows, rows, rows), span(base + lo, size, 128)]

    def h_send(r, col, b, part, where, name):
        ref = h_ref(slot(r, col, b), part, c)
        net.start(name, ref, ref, where)

    def to_mate(r, col, b, part):
        h_send(r, col, b, part, mate, ("m", r, col, b, part))

    def h_wait(r, col, b, part, when=None):
        net.wait(("x", r, col, b, part), h_ref(slot(r, col, b), part, c), when=when)

    def w_ref(yy, cc, j):
        return w_all.at[span((yy * 2 + cc) * depth, depth, depth), pl.ds(j * columns, columns)]

    def w_first(j, w):
        ref = w_ref(y, c, j)
        net.start(("w0", j), w, ref, at(xx=cross, cc=u), offset=c, width=2)
        net.start(("w0", j), w, ref, mate, offset=c, width=2, when=away)

    weights = (wq, wk, wv)
    mine = span(c * half, half, half)
    theirs = span((1 - c) * half, half, half)
    net.start(("x", 0, 0, 0, "f"), h_in.at[:, theirs], h_ref(slot(0, 0, 0), "f", 1 - c), mate, when=own)
    w_first(0, wq)
    there = z * SIDE + 2 * (1 - xl) + 1
    for hf in range(2):
        net.start(
            ("x", 0, 0, 1, "f"), h_in.at[:, pl.ds(hf * half, half)], h_ref(there, "f", hf),
            at(xx=cross, cc=hf), when=away,
        )
    w_first(1, wk)
    w_first(2, wv)
    net.start(("rate",), rates.at[0], rates.at[1], at(xx=cross))

    @pl.when(own)
    def _():
        h_all[span(slot(0, 0, 0) * rows, rows, rows), mine] = h_in[:, mine]
        for j in range(3):
            w_all[span(d * depth, depth, depth), j * columns : (j + 1) * columns] = weights[j][...]

    def spread(b):
        for way in (1, -1):
            h_send(0, 0, b, "f", zs[way], ("x", -way, 0, b, "f"))
        h_send(0, 0, b, "f", pair, ("x", 0, 1, b, "f"))
        to_mate(0, 0, b, "f")

    def w_spread(j):
        for cc in range(2):
            net.wait(("w0", j), w_ref(y, cc, j), offset=cc, width=2, when=jnp.logical_or(away, c != cc))
            for way in (1, -1):
                net.start(("w1", j, -way, cc), w_ref(y, cc, j), w_ref(y, cc, j), ys[way])

    def w_forward(j):
        for way, cc in ((1, 0), (-1, 1)):
            ref = w_ref(turned(y, -way), cc, j)
            net.wait(("w1", j, -way, cc), ref)
            net.start(("w2", j, cc), ref, ref, ys[way])

    def from_pair(b):
        h_wait(0, 1, b, "f")
        for way in (1, -1):
            h_send(0, 1, b, "a", zs[way], ("x", -way, 1, b, "a"))
        to_mate(0, 1, b, "f")

    def from_side(b):
        fast = 1 if b == 0 else -1
        for r in (-fast, fast):
            h_wait(r, 0, b, "f")
            if r == -fast:
                h_send(r, 0, b, "f", zs[fast], ("x", 2, 0, b, "f"))
            h_send(r, 0, b, "b", pair, ("x", r, 1, b, "b"))
            to_mate(r, 0, b, "f")

    def from_corner(b):
        fast = 1 if b == 0 else -1
        for r in (-fast, fast):
            h_wait(r, 1, b, "a")
            if r == -fast:
                h_send(r, 1, b, "a", zs[fast], ("x", 2, 1, b, "a"))
            to_mate(r, 1, b, "a")

    h_wait(0, 0, 0, "f", when=away)
    spread(0)
    w_spread(0)
    h_wait(0, 0, 1, "f")
    spread(1)
    w_spread(1)
    from_pair(0)
    from_side(0)
    w_spread(2)
    w_forward(0)
    from_pair(1)
    from_side(1)
    from_corner(0)
    w_forward(1)
    from_corner(1)
    for b in range(2):
        h_wait(2, 0, b, "f")
        h_send(2, 0, b, "b", pair, ("x", 2, 1, b, "b"))
        to_mate(2, 0, b, "f")
    w_forward(2)

    def c_send(hop, when=None):
        head = (s + hop) % blocks
        hz, hx = head // SIDE, head % SIDE
        far = (hx // 2 - c) * (hx // 2 - c)
        net.start(
            ("c",), c_in.at[:, span(head * columns, columns, columns)],
            c_all.at[span(s * rows, rows, rows)],
            {"sp": hz * SIDE + hx + far * (3 - 2 * hx), "dp": y * 2 + c + far * (1 - 2 * c)},
            offset=s, width=blocks, when=when,
        )

    c_send(0, when=away)
    for hop in range(1, blocks):
        c_send(hop)

    @pl.when(own)
    def _():
        c_all[span(s * rows, rows, rows), :] = c_in[:, span(s * columns, columns, columns)]

    for r in (-1, 1):
        for b in range(2):
            h_wait(r, 1, b, "b")
            to_mate(r, 1, b, "b")
    for b in range(2):
        h_wait(2, 1, b, "a")
        to_mate(2, 1, b, "a")
    for b in range(2):
        h_wait(2, 1, b, "b")
        to_mate(2, 1, b, "b")

    for j in range(3):
        for way, cc in ((1, 1), (-1, 0)):
            net.wait(("w1", j, -way, cc), w_ref(turned(y, -way), cc, j))
        for cc in range(2):
            net.wait(("w2", j, cc), w_ref(turned(y, 2), cc, j))

    def mate_wait(r):
        for col in range(2):
            for b in range(2):
                for part in ("f",) if col == 0 or r == 0 else ("a", "b"):
                    net.wait(("m", r, col, b, part), h_ref(slot(r, col, b), part, 1 - c))

    def project(r, j):
        place = span(turned(z, r) * four, four, four)
        cols = span(j * columns, columns, columns)
        value = dot(h_all[place, :], w_all[:, cols]).astype(BF16)
        factor = jnp.where(j == 1, scale, 1.0).astype(F32)
        p_all[place, cols] = (value.astype(F32) * factor).astype(BF16)

    for r in (0, 1, -1):
        mate_wait(r)

    @pl.loop(0, 9)
    def _(t):
        o = t // 3
        project(o + o // 2, t % 3)

    mate_wait(2)

    @pl.loop(0, 3)
    def _(j):
        project(2, j)

    net.wait(("rate",), rates.at[1])
    for k in range(blocks):
        source = (s + k) % blocks
        net.wait(
            ("c",), c_all.at[span(source * rows, rows, rows)], offset=source, width=blocks,
            when=away if k == 0 else None,
        )

    pick = jnp.where(own, 1.0, 0.0).astype(F32)
    g = rates[0] * pick + rates[1] * (1.0 - pick)
    g_row = g[0:1, :]
    gap = (
        lax.broadcasted_iota(jnp.int32, (BLOCK, BLOCK), 0) - lax.broadcasted_iota(jnp.int32, (BLOCK, BLOCK), 1)
    ).astype(F32)
    place = lax.broadcasted_iota(jnp.int32, (BLOCK, columns), 0).astype(F32)
    g_sq = g_row[:, :BLOCK]
    inner[...] = jnp.where(gap >= 0, jnp.exp(g_sq * jnp.maximum(gap, 0.0)), 0.0)
    inner_t[...] = jnp.where(gap <= 0, jnp.exp(g_sq * jnp.maximum(-gap, 0.0)), 0.0)
    decays[0] = jnp.exp(g_row * (place + 1.0))
    decays[1] = jnp.exp(g_row * (BLOCK - 1.0 - place))
    block_decay = jnp.exp(g_row * BLOCK)
    state[...] = jnp.zeros_like(state)
    back[...] = jnp.zeros_like(back)
    parts = [slice(j * columns, (j + 1) * columns) for j in range(3)]

    def slot_of(i):
        iz, ix = i // SIDE, i % SIDE
        b = (ix // 2 - u) * (ix // 2 - u)
        return iz * SIDE + 2 * (ix + b * (3 - 2 * ix) - 2 * u) + b

    @pl.loop(0, blocks)
    def _(i):
        put = span(slot_of(i) * BLOCK, BLOCK, BLOCK)
        k, v = p_all[put, parts[1]], p_all[put, parts[2]]
        ct = c_all[span(i * BLOCK, BLOCK, BLOCK), :]
        mixed = (dot(ct, v, NT) * inner[...]).astype(BF16)
        held = state[...]
        grad_q = dot(mixed, k) + dot(ct, held.astype(BF16), NT) * decays[0]
        weighted = (k.astype(F32) * decays[1]).astype(BF16)
        state[...] = held * block_decay + dot(weighted, v, TN)
        g_all[put, parts[0]] = grad_q.astype(BF16)

        i = blocks - 1 - i
        put = span(slot_of(i) * BLOCK, BLOCK, BLOCK)
        q, k, v = (p_all[put, part] for part in parts)
        ct = c_all[span(i * BLOCK, BLOCK, BLOCK), :]
        mixed_t = (dot(v, ct, NT) * inner_t[...]).astype(BF16)
        scores_t = (dot(k, q, NT) * inner_t[...]).astype(BF16)
        held = back[...]
        held_bf = held.astype(BF16)
        grad_v = dot(scores_t, ct) + dot(k, held_bf) * decays[1]
        grad_k = (dot(mixed_t, q) + dot(v, held_bf, NT) * decays[1]) * scale
        weighted = (q.astype(F32) * decays[0]).astype(BF16)
        back[...] = held * block_decay + dot(weighted, ct, TN)
        g_all[put, parts[1]] = grad_k.astype(BF16)
        g_all[put, parts[2]] = grad_v.astype(BF16)

    alpha, beta = pl.ds(0, FIRST), pl.ds(FIRST, half - FIRST)
    chunk = half // 2

    def r_rows(r):
        return span(turned(z, r) * four, four, four)

    def pick_rows(r, hf):
        return span(turned(z, r) * four + hf * two, two, two)

    def other(r):
        lhs_rows = r_rows(r)

        @pl.loop(0, 2)
        def _(i):
            value = dot(g_all[lhs_rows, :], w_all[span((1 - c) * half + i * chunk, chunk, chunk), :], NT)
            pout[lhs_rows, span(i * chunk, chunk, chunk)] = value.astype(BF16)

        net.start(("p", r), pout.at[lhs_rows], pin.at[lhs_rows], mate)

    def summed(r):
        lhs_rows = r_rows(r)
        net.wait(("p", r), pin.at[lhs_rows])

        @pl.loop(0, 2)
        def _(i):
            value = dot(g_all[lhs_rows, :], w_all[span(c * half + i * chunk, chunk, chunk), :], NT)
            cols = span(i * chunk, chunk, chunk)
            psum[lhs_rows, cols] = (value + pin[lhs_rows, cols].astype(F32)).astype(BF16)

        net.start(("b0", r), psum.at[pick_rows(r, 1 - xl), beta], rb0.at[r % SIDE], pair)

    def add(place, cols, *refs):
        total = psum[place, cols].astype(F32)
        for ref in refs:
            total = total + ref.astype(F32)
        psum[place, cols] = total.astype(BF16)

    def alpha_send(r, hf, way, name, dst):
        net.start(name, psum.at[pick_rows(r, hf), alpha], dst, zs[way])

    def b_rows(r, b):
        return span(turned(z, r) * four + xl * two + b * rows, rows, rows)

    def beta_send(r, b, way, name, dst):
        net.start(name, psum.at[b_rows(r, b), beta], dst, zs[way])

    def a2(e, hf):
        return ra2.at[e, pl.ds(hf * two, two)]

    def b2(e, b):
        return rb2.at[e, pl.ds(b * rows, rows)]

    def w_grad(r, hf):
        cols = span((turned(y, r) * 2 + hf) * depth, depth, depth)
        return dot(h_all[:, cols], g_all[...], TN)

    def y2(e, hf):
        return yr2.at[e, pl.ds(hf * depth, depth)]

    other(2)

    @pl.loop(0, 2)
    def _(hf):
        ysend[hf] = w_grad(2, hf).astype(BF16)

    net.start(("y1", 0), ysend.at[0], yr1.at[0], ys[1])
    net.start(("y1", 1), ysend.at[1], yr1.at[1], ys[-1])
    summed(2)
    alpha_send(2, 0, 1, ("a1", 0), ra1.at[0])
    alpha_send(2, 1, -1, ("a1", 1), ra1.at[1])
    other(1)
    other(-1)
    summed(1)
    alpha_send(1, 1, 1, ("a2", 0, 1), a2(0, 1))
    summed(-1)
    alpha_send(-1, 0, -1, ("a2", 1, 0), a2(1, 0))

    @pl.loop(0, 2)
    def _(e):
        yone[e, 1 - e] = w_grad(1 + 2 * e, 1 - e).astype(BF16)

    net.start(("y2", 0, 1), yone.at[0, 1], y2(0, 1), ys[1])
    net.start(("y2", 1, 0), yone.at[1, 0], y2(1, 0), ys[-1])
    other(0)

    net.wait(("a1", 0), ra1.at[0])
    add(pick_rows(1, 0), alpha, ra1[0])
    alpha_send(1, 0, 1, ("a2", 0, 0), a2(0, 0))
    net.wait(("a1", 1), ra1.at[1])
    add(pick_rows(-1, 1), alpha, ra1[1])
    alpha_send(-1, 1, -1, ("a2", 1, 1), a2(1, 1))

    net.wait(("b0", 2), rb0.at[2])
    add(pick_rows(2, xl), beta, rb0[2])
    beta_send(2, 0, 1, ("b1", 0), rb1.at[0])
    beta_send(2, 1, -1, ("b1", 1), rb1.at[1])
    summed(0)

    @pl.loop(0, 2)
    def _(e):
        ykeep[e] = w_grad(1 + 2 * e, e)

    for e, way in ((0, 1), (1, -1)):
        net.wait(("y1", e), yr1.at[e])
        yone[e, e] = (ykeep[e] + yr1[e].astype(F32)).astype(BF16)
        net.start(("y2", e, e), yone.at[e, e], y2(e, e), ys[way])

    for r, b, way, e in ((1, 1, 1, 0), (-1, 0, -1, 1)):
        net.wait(("b0", r), rb0.at[r % SIDE])
        add(pick_rows(r, xl), beta, rb0[r % SIDE])
        beta_send(r, b, way, ("b2", e, b), b2(e, b))

    @pl.loop(0, 2)
    def _(hf):
        yhome[hf] = w_grad(0, hf)

    for r, b, way, e in ((1, 0, 1, 0), (-1, 1, -1, 1)):
        net.wait(("b1", e), rb1.at[e])
        add(b_rows(r, b), beta, rb1[e])
        beta_send(r, b, way, ("b2", e, b), b2(e, b))
    net.wait(("b0", 0), rb0.at[0])
    add(pick_rows(0, xl), beta, rb0[0])

    for e, hf in ((0, 1), (1, 0), (0, 0), (1, 1)):
        net.wait(("a2", e, hf), a2(e, hf))
    for hf in range(2):
        add(pick_rows(0, hf), alpha, ra2[0, hf * two : (hf + 1) * two], ra2[1, hf * two : (hf + 1) * two])
    net.start(("a3",), psum.at[pick_rows(0, 1 - xl), alpha], ra3, pair)

    def deliver(cols):
        lo = cols.start
        dst = dbuf.at[c, :, cols]
        net.start(("d", lo), psum.at[b_rows(0, 1), cols], dst, at(xx=cross, cc=u), offset=c, width=2)
        net.start(("d", lo), psum.at[b_rows(0, 0), cols], dst, mate, offset=c, width=2, when=away)

    for e, b in ((0, 1), (1, 0), (0, 0), (1, 1)):
        net.wait(("b2", e, b), b2(e, b))
    add(pick_rows(0, xl), beta, rb2[0], rb2[1])
    deliver(beta)

    for e, hf in ((0, 1), (1, 0), (0, 0), (1, 1)):
        net.wait(("y2", e, hf), y2(e, hf))
    for hf in range(2):
        lanes = slice(hf * depth, (hf + 1) * depth)
        total = yhome[hf] + yr2[0, lanes].astype(F32) + yr2[1, lanes].astype(F32)
        yhome[hf] = total
        yout[hf] = total.astype(BF16)
    net.start(("e", 0), yout.at[1 - c], yend.at[0], mate, when=own)
    for hf in range(2):
        net.start(("e", 1), yout.at[hf], yend.at[1], at(xx=cross, cc=hf), when=away)

    net.wait(("a3",), ra3)
    add(pick_rows(0, xl), alpha, ra3[...])
    deliver(alpha)

    net.wait(("e", 1), yend.at[1], when=own)
    net.wait(("e", 0), yend.at[0], when=away)
    net.wait(("e", 1), yend.at[1], when=away)

    @pl.when(own)
    def _():
        for j, out in enumerate((dq, dk, dv)):
            out[...] = (yhome[c, :, parts[j]] + yend[1, :, parts[j]].astype(F32)) * 0.125

    @pl.when(away)
    def _():
        for j, out in enumerate((dq, dk, dv)):
            out[...] = (yend[0, :, parts[j]].astype(F32) + yend[1, :, parts[j]].astype(F32)) * 0.125

    for cols in (beta, alpha):
        for hf in range(2):
            net.wait(
                ("d", cols.start), dbuf.at[hf, :, cols], offset=hf, width=2, when=jnp.logical_or(away, c != hf)
            )

    @pl.when(own)
    def _():
        dbuf[c] = psum[b_rows(0, 0), :]

    for hf in range(2):
        dh[:, hf * half : (hf + 1) * half] = dbuf[hf]
    net.drain()


def whole(rate, h, c, wq, wk, wv):
    rows, width = h.shape
    depth, columns = wq.shape
    blocks = SIDE * SIDE
    length = rows * blocks
    half = width // 2
    rest = half - FIRST
    vmem = pl.BlockSpec(memory_space=pltpu.VMEM)
    dma = pltpu.SemaphoreType.DMA

    def buf(*shape, kind=BF16):
        return pltpu.VMEM(shape, kind)

    return pl.pallas_call(
        whole_kernel,
        out_shape=(buf(rows, width),) + (buf(depth, columns, kind=F32),) * 3,
        in_specs=[pl.BlockSpec(memory_space=pltpu.SMEM)] + [vmem] * 5,
        out_specs=(vmem,) * 4,
        scratch_shapes=[
            buf(length, width),
            buf(length, columns),
            buf(depth * 8, 3 * columns),
            buf(length, 3 * columns),
            buf(length, 3 * columns),
            buf(columns, columns, kind=F32),
            buf(columns, columns, kind=F32),
            buf(2, 8, columns, kind=F32),
            buf(BLOCK, BLOCK, kind=F32),
            buf(BLOCK, BLOCK, kind=F32),
            buf(2, BLOCK, columns, kind=F32),
            buf(length, half),
            buf(length, half),
            buf(length, half),
            buf(2, 2 * rows, FIRST),
            buf(2, 4 * rows, FIRST),
            buf(2 * rows, FIRST),
            buf(SIDE, 2 * rows, rest),
            buf(2, rows, rest),
            buf(2, 2 * rows, rest),
            buf(2, rows, half),
            buf(2, depth, 3 * columns),
            buf(2, 2, depth, 3 * columns),
            buf(2, depth, 3 * columns, kind=F32),
            buf(2, depth, 3 * columns, kind=F32),
            buf(2, depth, 3 * columns),
            buf(2, 2 * depth, 3 * columns),
            buf(2, depth, 3 * columns),
            buf(2, depth, 3 * columns),
            dma((SEMS,)),
            dma((SEMS,)),
        ],
        compiler_params=pltpu.CompilerParams(
            collective_id=0, has_side_effects=True, vmem_limit_bytes=VMEM_LIMIT
        ),
        name="whole",
    )(rate, h, c, wq, wk, wv)


def finish_kernel(count, *refs):
    ins, outs, sems = refs[:count], refs[count : 2 * count], refs[2 * count]
    moves = [pltpu.make_async_copy(ins[i], outs[i], sems.at[i]) for i in range(count)]
    for move in moves:
        move.start()
    for move in moves:
        move.wait()


def finish(*arrays):
    count = len(arrays)
    return pl.pallas_call(
        functools.partial(finish_kernel, count),
        out_shape=tuple(jax.ShapeDtypeStruct(a.shape, a.dtype) for a in arrays),
        in_specs=[pl.BlockSpec(memory_space=pltpu.VMEM)] * count,
        out_specs=(pl.BlockSpec(memory_space=pl.ANY),) * count,
        scratch_shapes=[pltpu.SemaphoreType.DMA((count,))],
        compiler_params=pltpu.CompilerParams(vmem_limit_bytes=4 * 1024 * 1024),
        name="finish",
    )(*arrays)


def body(hidden_in, mix_cotangent, query_weight, key_weight, value_weight, decay_log):
    dh, dq, dk, dv = finish(
        *whole(decay_log, hidden_in[0], mix_cotangent[0], query_weight, key_weight, value_weight)
    )
    return dh[None], dq, dk, dv


def solution(mesh):
    placed = (
        P("dp", "sp", None),
        P("dp", "sp", None),
        P("dp", "sp"),
        P("dp", "sp"),
        P("dp", "sp"),
        P("sp"),
    )
    return jax.shard_map(
        body,
        mesh=mesh,
        in_specs=placed,
        out_specs=(P("dp", "sp", None), P("dp", "sp"), P("dp", "sp"), P("dp", "sp")),
        check_vma=False,
    )
```

time: 431 us -> 127 us (0.29)
  Pallas kernels: 426 us -> 125 us
    pallas_call x1, Pallas kernels: 425 us -> 124 us  [whole(): pl.pallas_call(whole_kernel, out_shape=(buf(rows, width),) + (buf(depth,...]
where the time goes in v1:
time: 127 us
  Pallas kernels  125 us (98%)
  between operations  1.29 us (1%)
    pallas_call x1, Pallas kernels, whole(): pl.pallas_call(whole_kernel, out_shape=(buf(rows, width),) + (buf(depth,...  124 us

profile of v1, /device:TPU:1, one launch (start us, length us, event | category | flops | bytes accessed | tf_op | source)
XLA Modules:
  0.0 126.8 jit_solution(290495762101378309)
XLA Ops:
  1.3 124.4 %whole.1 = (bf16[128,2048]{1,0:T(8,128)(2,1)S(1)}, f32[256,256]{1,0:T(8,128)S(1)}, f32[256,256]{1,0:T(8,128)S(1)}, f32[256,256]{1,0:T(8,128)S(1)}) custom-call(f32[1]{0:T(128)S(6)} %copy.10.rate, bf16[128,2048]{1,0:T(8,128)(2,1)} %bitcast.4, bf16[128,4096]{1,0:T(8,128)(2,1)} %bitcast.3, bf16[256,256]{1,0:T(8,128)(2,1)} %wq.1, bf16[256,256]{1,0:T(8,128)(2,1)} %wk.1, ...), custom_call_target="tpu_custom_call" | custom-call | tf_op jit(solution)/shard_map/whole/pallas_call | solution.py:553
  125.7 1.1 finish.1

commit v2 on v1

--- a/solution.py
+++ b/solution.py
@@ -10,6 +10,7 @@
 BLOCK = 128
 SIDE = 4
 FIRST = 640
+EARLY = 384
 F32 = jnp.float32
 BF16 = jnp.bfloat16
 MESH = pl.DeviceIdType.MESH
@@ -17,7 +18,7 @@
 NT = (((1,), (1,)), ((), ()))
 TN = (((0,), (0,)), ((), ()))
 VMEM_LIMIT = 60 * 1024 * 1024
-SEMS = 160
+SEMS = 256
 
 
 def dot(a, b, dims=NN):
@@ -79,9 +80,9 @@
 
 def whole_kernel(
     rate, h_in, c_in, wq, wk, wv, dh, dq, dk, dv,
-    h_all, c_all, w_all, p_all, g_all, state, back, rates, inner, inner_t, decays,
+    h_all, c_all, w_all, p_all, g_all, g_turn, state, back, rates, inner, inner_t, decays,
     pout, pin, psum, ra1, ra2, ra3, rb0, rb1, rb2, dbuf,
-    ysend, yone, ykeep, yhome, yr1, yr2, yout, yend, send, recv,
+    ysend, yone, yhome, yr1, yr2, yout, yend, send, recv,
 ):
     s = lax.axis_index("sp")
     d = lax.axis_index("dp")
@@ -113,6 +114,7 @@
     ys = {1: at(yy=turned(y, 1)), -1: at(yy=turned(y, -1))}
     cross = 3 - x
     net = Net(send, recv, mate)
+    weights = (wq, wk, wv)
 
     barrier = pltpu.get_barrier_semaphore()
     peers = [mate, ys[1], ys[-1]]
@@ -145,24 +147,25 @@
     def w_ref(yy, cc, j):
         return w_all.at[span((yy * 2 + cc) * depth, depth, depth), pl.ds(j * columns, columns)]
 
-    def w_first(j, w):
-        ref = w_ref(y, c, j)
-        net.start(("w0", j), w, ref, at(xx=cross, cc=u), offset=c, width=2)
-        net.start(("w0", j), w, ref, mate, offset=c, width=2, when=away)
-
-    weights = (wq, wk, wv)
+    def w_near(j):
+        net.start(("w0", j), weights[j], w_ref(y, c, j), mate, offset=c, width=2, when=away)
+
+    def w_cross(j, who):
+        net.start(("w0", j), weights[j], w_ref(y, c, j), at(xx=cross, cc=u), offset=c, width=2, when=who)
+
     mine = span(c * half, half, half)
     theirs = span((1 - c) * half, half, half)
     net.start(("x", 0, 0, 0, "f"), h_in.at[:, theirs], h_ref(slot(0, 0, 0), "f", 1 - c), mate, when=own)
-    w_first(0, wq)
     there = z * SIDE + 2 * (1 - xl) + 1
     for hf in range(2):
         net.start(
             ("x", 0, 0, 1, "f"), h_in.at[:, pl.ds(hf * half, half)], h_ref(there, "f", hf),
             at(xx=cross, cc=hf), when=away,
         )
-    w_first(1, wk)
-    w_first(2, wv)
+    for j in range(3):
+        w_near(j)
+    for j in range(3):
+        w_cross(j, away)
     net.start(("rate",), rates.at[0], rates.at[1], at(xx=cross))
 
     @pl.when(own)
@@ -177,17 +180,18 @@
         h_send(0, 0, b, "f", pair, ("x", 0, 1, b, "f"))
         to_mate(0, 0, b, "f")
 
-    def w_spread(j):
+    def w_spread(j, who):
         for cc in range(2):
-            net.wait(("w0", j), w_ref(y, cc, j), offset=cc, width=2, when=jnp.logical_or(away, c != cc))
+            far = who if who is away else jnp.logical_and(own, c != cc)
+            net.wait(("w0", j), w_ref(y, cc, j), offset=cc, width=2, when=far)
             for way in (1, -1):
-                net.start(("w1", j, -way, cc), w_ref(y, cc, j), w_ref(y, cc, j), ys[way])
-
-    def w_forward(j):
+                net.start(("w1", j, -way, cc), w_ref(y, cc, j), w_ref(y, cc, j), ys[way], when=who)
+
+    def w_forward(j, who):
         for way, cc in ((1, 0), (-1, 1)):
             ref = w_ref(turned(y, -way), cc, j)
-            net.wait(("w1", j, -way, cc), ref)
-            net.start(("w2", j, cc), ref, ref, ys[way])
+            net.wait(("w1", j, -way, cc), ref, when=who)
+            net.start(("w2", j, cc), ref, ref, ys[way], when=who)
 
     def from_pair(b):
         h_wait(0, 1, b, "f")
@@ -212,26 +216,35 @@
                 h_send(r, 1, b, "a", zs[fast], ("x", 2, 1, b, "a"))
             to_mate(r, 1, b, "a")
 
-    h_wait(0, 0, 0, "f", when=away)
-    spread(0)
-    w_spread(0)
-    h_wait(0, 0, 1, "f")
-    spread(1)
-    w_spread(1)
-    from_pair(0)
-    from_side(0)
-    w_spread(2)
-    w_forward(0)
-    from_pair(1)
-    from_side(1)
-    from_corner(0)
-    w_forward(1)
-    from_corner(1)
-    for b in range(2):
+    def from_far(b):
         h_wait(2, 0, b, "f")
         h_send(2, 0, b, "b", pair, ("x", 2, 1, b, "b"))
         to_mate(2, 0, b, "f")
-    w_forward(2)
+
+    h_wait(0, 0, 0, "f", when=away)
+    spread(0)
+    for j in range(3):
+        w_spread(j, own)
+    h_wait(0, 0, 1, "f")
+    spread(1)
+    for j in range(3):
+        w_cross(j, own)
+    from_side(0)
+    from_pair(0)
+    w_forward(0, own)
+    w_spread(0, away)
+    from_side(1)
+    from_pair(1)
+    w_forward(1, own)
+    w_spread(1, away)
+    w_forward(2, own)
+    w_spread(2, away)
+    from_far(0)
+    from_corner(0)
+    w_forward(0, away)
+    from_far(1)
+    from_corner(1)
+    w_forward(1, away)
 
     def c_send(hop, when=None):
         head = (s + hop) % blocks
@@ -256,6 +269,7 @@
         for b in range(2):
             h_wait(r, 1, b, "b")
             to_mate(r, 1, b, "b")
+    w_forward(2, away)
     for b in range(2):
         h_wait(2, 1, b, "a")
         to_mate(2, 1, b, "a")
@@ -336,7 +350,9 @@
         grad_q = dot(mixed, k) + dot(ct, held.astype(BF16), NT) * decays[0]
         weighted = (k.astype(F32) * decays[1]).astype(BF16)
         state[...] = held * block_decay + dot(weighted, v, TN)
-        g_all[put, parts[0]] = grad_q.astype(BF16)
+        grad_q = grad_q.astype(BF16)
+        g_all[put, parts[0]] = grad_q
+        g_turn[parts[0], put] = grad_q.T
 
         i = blocks - 1 - i
         put = span(slot_of(i) * BLOCK, BLOCK, BLOCK)
@@ -350,10 +366,12 @@
         grad_k = (dot(mixed_t, q) + dot(v, held_bf, NT) * decays[1]) * scale
         weighted = (q.astype(F32) * decays[0]).astype(BF16)
         back[...] = held * block_decay + dot(weighted, ct, TN)
-        g_all[put, parts[1]] = grad_k.astype(BF16)
-        g_all[put, parts[2]] = grad_v.astype(BF16)
-
-    alpha, beta = pl.ds(0, FIRST), pl.ds(FIRST, half - FIRST)
+        for part, grad in ((parts[1], grad_k.astype(BF16)), (parts[2], grad_v.astype(BF16))):
+            g_all[put, part] = grad
+            g_turn[part, put] = grad.T
+
+    pieces = (pl.ds(0, EARLY), pl.ds(EARLY, FIRST - EARLY))
+    beta = pl.ds(FIRST, half - FIRST)
     chunk = half // 2
 
     def r_rows(r):
@@ -390,97 +408,38 @@
             total = total + ref.astype(F32)
         psum[place, cols] = total.astype(BF16)
 
-    def alpha_send(r, hf, way, name, dst):
-        net.start(name, psum.at[pick_rows(r, hf), alpha], dst, zs[way])
-
-    def b_rows(r, b):
-        return span(turned(z, r) * four + xl * two + b * rows, rows, rows)
-
-    def beta_send(r, b, way, name, dst):
-        net.start(name, psum.at[b_rows(r, b), beta], dst, zs[way])
-
-    def a2(e, hf):
-        return ra2.at[e, pl.ds(hf * two, two)]
-
-    def b2(e, b):
-        return rb2.at[e, pl.ds(b * rows, rows)]
-
-    def w_grad(r, hf):
-        cols = span((turned(y, r) * 2 + hf) * depth, depth, depth)
-        return dot(h_all[:, cols], g_all[...], TN)
-
-    def y2(e, hf):
-        return yr2.at[e, pl.ds(hf * depth, depth)]
-
-    other(2)
-
-    @pl.loop(0, 2)
-    def _(hf):
-        ysend[hf] = w_grad(2, hf).astype(BF16)
-
-    net.start(("y1", 0), ysend.at[0], yr1.at[0], ys[1])
-    net.start(("y1", 1), ysend.at[1], yr1.at[1], ys[-1])
-    summed(2)
-    alpha_send(2, 0, 1, ("a1", 0), ra1.at[0])
-    alpha_send(2, 1, -1, ("a1", 1), ra1.at[1])
-    other(1)
-    other(-1)
-    summed(1)
-    alpha_send(1, 1, 1, ("a2", 0, 1), a2(0, 1))
-    summed(-1)
-    alpha_send(-1, 0, -1, ("a2", 1, 0), a2(1, 0))
-
-    @pl.loop(0, 2)
-    def _(e):
-        yone[e, 1 - e] = w_grad(1 + 2 * e, 1 - e).astype(BF16)
-
-    net.start(("y2", 0, 1), yone.at[0, 1], y2(0, 1), ys[1])
-    net.start(("y2", 1, 0), yone.at[1, 0], y2(1, 0), ys[-1])
-    other(0)
-
-    net.wait(("a1", 0), ra1.at[0])
-    add(pick_rows(1, 0), alpha, ra1[0])
-    alpha_send(1, 0, 1, ("a2", 0, 0), a2(0, 0))
-    net.wait(("a1", 1), ra1.at[1])
-    add(pick_rows(-1, 1), alpha, ra1[1])
-    alpha_send(-1, 1, -1, ("a2", 1, 1), a2(1, 1))
-
-    net.wait(("b0", 2), rb0.at[2])
-    add(pick_rows(2, xl), beta, rb0[2])
-    beta_send(2, 0, 1, ("b1", 0), rb1.at[0])
-    beta_send(2, 1, -1, ("b1", 1), rb1.at[1])
-    summed(0)
-
-    @pl.loop(0, 2)
-    def _(e):
-        ykeep[e] = w_grad(1 + 2 * e, e)
-
-    for e, way in ((0, 1), (1, -1)):
-        net.wait(("y1", e), yr1.at[e])
-        yone[e, e] = (ykeep[e] + yr1[e].astype(F32)).astype(BF16)
-        net.start(("y2", e, e), yone.at[e, e], y2(e, e), ys[way])
-
-    for r, b, way, e in ((1, 1, 1, 0), (-1, 0, -1, 1)):
-        net.wait(("b0", r), rb0.at[r % SIDE])
-        add(pick_rows(r, xl), beta, rb0[r % SIDE])
-        beta_send(r, b, way, ("b2", e, b), b2(e, b))
-
-    @pl.loop(0, 2)
-    def _(hf):
-        yhome[hf] = w_grad(0, hf)
-
-    for r, b, way, e in ((1, 0, 1, 0), (-1, 1, -1, 1)):
-        net.wait(("b1", e), rb1.at[e])
-        add(b_rows(r, b), beta, rb1[e])
-        beta_send(r, b, way, ("b2", e, b), b2(e, b))
-    net.wait(("b0", 0), rb0.at[0])
-    add(pick_rows(0, xl), beta, rb0[0])
-
-    for e, hf in ((0, 1), (1, 0), (0, 0), (1, 1)):
-        net.wait(("a2", e, hf), a2(e, hf))
-    for hf in range(2):
-        add(pick_rows(0, hf), alpha, ra2[0, hf * two : (hf + 1) * two], ra2[1, hf * two : (hf + 1) * two])
-    net.start(("a3",), psum.at[pick_rows(0, 1 - xl), alpha], ra3, pair)
+    def a1(i, e):
+        return ra1.at[e, :, pieces[i]]
+
+    def a2(i, e, hf):
+        return ra2.at[e, pl.ds(hf * two, two), pieces[i]]
+
+    def a3(i):
+        return ra3.at[:, pieces[i]]
+
+    def alpha_send(i, r, hf, way, name, dst):
+        net.start(name, psum.at[pick_rows(r, hf), pieces[i]], dst, zs[way])
+
+    def alpha_first(i):
+        alpha_send(i, 2, 0, 1, ("a1", i, 0), a1(i, 0))
+        alpha_send(i, 2, 1, -1, ("a1", i, 1), a1(i, 1))
+
+    def alpha_plain(i, r):
+        e = 0 if r == 1 else 1
+        alpha_send(i, r, 1 - e, r, ("a2", i, e, 1 - e), a2(i, e, 1 - e))
+
+    def alpha_added(i):
+        for e, r in ((0, 1), (1, -1)):
+            net.wait(("a1", i, e), a1(i, e))
+            add(pick_rows(r, e), pieces[i], a1(i, e)[...])
+            alpha_send(i, r, e, r, ("a2", i, e, e), a2(i, e, e))
+
+    def alpha_last(i):
+        for e, hf in ((0, 1), (1, 0), (0, 0), (1, 1)):
+            net.wait(("a2", i, e, hf), a2(i, e, hf))
+        for hf in range(2):
+            add(pick_rows(0, hf), pieces[i], a2(i, 0, hf)[...], a2(i, 1, hf)[...])
+        net.start(("a3", i), psum.at[pick_rows(0, 1 - xl), pieces[i]], a3(i), pair)
 
     def deliver(cols):
         lo = cols.start
@@ -488,41 +447,137 @@
         net.start(("d", lo), psum.at[b_rows(0, 1), cols], dst, at(xx=cross, cc=u), offset=c, width=2)
         net.start(("d", lo), psum.at[b_rows(0, 0), cols], dst, mate, offset=c, width=2, when=away)
 
-    for e, b in ((0, 1), (1, 0), (0, 0), (1, 1)):
-        net.wait(("b2", e, b), b2(e, b))
-    add(pick_rows(0, xl), beta, rb2[0], rb2[1])
-    deliver(beta)
-
-    for e, hf in ((0, 1), (1, 0), (0, 0), (1, 1)):
-        net.wait(("y2", e, hf), y2(e, hf))
-    for hf in range(2):
-        lanes = slice(hf * depth, (hf + 1) * depth)
-        total = yhome[hf] + yr2[0, lanes].astype(F32) + yr2[1, lanes].astype(F32)
-        yhome[hf] = total
-        yout[hf] = total.astype(BF16)
-    net.start(("e", 0), yout.at[1 - c], yend.at[0], mate, when=own)
-    for hf in range(2):
-        net.start(("e", 1), yout.at[hf], yend.at[1], at(xx=cross, cc=hf), when=away)
-
-    net.wait(("a3",), ra3)
-    add(pick_rows(0, xl), alpha, ra3[...])
-    deliver(alpha)
-
-    net.wait(("e", 1), yend.at[1], when=own)
-    net.wait(("e", 0), yend.at[0], when=away)
-    net.wait(("e", 1), yend.at[1], when=away)
+    def alpha_deliver(i):
+        net.wait(("a3", i), a3(i))
+        add(pick_rows(0, xl), pieces[i], a3(i)[...])
+        deliver(pieces[i])
+
+    def b_rows(r, b):
+        return span(turned(z, r) * four + xl * two + b * rows, rows, rows)
+
+    def b2(e, b):
+        return rb2.at[e, pl.ds(b * rows, rows)]
+
+    def beta_send(r, b, way, name, dst):
+        net.start(name, psum.at[b_rows(r, b), beta], dst, zs[way])
+
+    def beta_take(r):
+        net.wait(("b0", r), rb0.at[r % SIDE])
+        add(pick_rows(r, xl), beta, rb0[r % SIDE])
+
+    def beta_first():
+        beta_take(2)
+        beta_send(2, 0, 1, ("b1", 0), rb1.at[0])
+        beta_send(2, 1, -1, ("b1", 1), rb1.at[1])
+
+    def beta_plain():
+        for r, b, e in ((1, 1, 0), (-1, 0, 1)):
+            beta_take(r)
+            beta_send(r, b, r, ("b2", e, b), b2(e, b))
+
+    def beta_added():
+        for r, b, e in ((1, 0, 0), (-1, 1, 1)):
+            net.wait(("b1", e), rb1.at[e])
+            add(b_rows(r, b), beta, rb1[e])
+            beta_send(r, b, r, ("b2", e, b), b2(e, b))
+
+    def beta_last():
+        beta_take(0)
+        for e, b in ((0, 1), (1, 0), (0, 0), (1, 1)):
+            net.wait(("b2", e, b), b2(e, b))
+        add(pick_rows(0, xl), beta, rb2[0], rb2[1])
+        deliver(beta)
+
+    lanes = [pl.ds(hf * depth, depth) for hf in range(2)]
+
+    def w_grad(r, j):
+        cols = span(turned(y, r) * 2 * depth, 2 * depth, depth)
+        return dot(g_turn[parts[j], :], h_all[:, cols])
+
+    def y_first(j):
+        ysend[j] = w_grad(2, j).astype(BF16)
+        for e, way in ((0, 1), (1, -1)):
+            net.start(("y1", j, e), ysend.at[j, :, lanes[e]], yr1.at[j, e], ys[way])
+
+    def y2(j, e, hf):
+        return yr2.at[j, e, :, lanes[hf]]
+
+    def y_second(j):
+        for e, r in ((0, 1), (1, -1)):
+            value = w_grad(r, j)
+            keep = value[:, e * depth : (e + 1) * depth]
+            yone[j, e, :, lanes[1 - e]] = value[:, (1 - e) * depth : (2 - e) * depth].astype(BF16)
+            net.start(("y2", j, e, 1 - e), yone.at[j, e, :, lanes[1 - e]], y2(j, e, 1 - e), ys[r])
+            net.wait(("y1", j, e), yr1.at[j, e])
+            yone[j, e, :, lanes[e]] = (keep + yr1[j, e].astype(F32)).astype(BF16)
+            net.start(("y2", j, e, e), yone.at[j, e, :, lanes[e]], y2(j, e, e), ys[r])
+
+    def y_home(j):
+        yhome[j] = w_grad(0, j)
+
+    def y_last(j):
+        for e, hf in ((0, 1), (1, 0), (0, 0), (1, 1)):
+            net.wait(("y2", j, e, hf), y2(j, e, hf))
+        total = yhome[j] + yr2[j, 0].astype(F32) + yr2[j, 1].astype(F32)
+        yhome[j] = total
+        yout[j] = total.astype(BF16)
+        half_of = span((1 - c) * depth, depth, depth)
+        net.start(("e", j, 0), yout.at[j, :, half_of], yend.at[j, 0], mate, when=own)
+        for hf in range(2):
+            net.start(("e", j, 1), yout.at[j, :, lanes[hf]], yend.at[j, 1], at(xx=cross, cc=hf), when=away)
+
+    other(2)
+    y_first(0)
+    y_first(1)
+    summed(2)
+    alpha_first(0)
+    alpha_first(1)
+    other(1)
+    y_first(2)
+    other(-1)
+    summed(1)
+    alpha_plain(0, 1)
+    summed(-1)
+    alpha_plain(0, -1)
+    y_second(0)
+    alpha_added(0)
+    alpha_plain(1, 1)
+    alpha_plain(1, -1)
+    other(0)
+    y_second(1)
+    alpha_added(1)
+    beta_first()
+    summed(0)
+    y_second(2)
+    beta_plain()
+    for j in range(3):
+        y_home(j)
+    y_last(0)
+    alpha_last(0)
+    y_last(1)
+    alpha_last(1)
+    alpha_deliver(0)
+    beta_added()
+    y_last(2)
+    alpha_deliver(1)
+    beta_last()
+
+    for j in range(3):
+        net.wait(("e", j, 1), yend.at[j, 1])
+        net.wait(("e", j, 0), yend.at[j, 0], when=away)
 
     @pl.when(own)
     def _():
+        here = span(c * depth, depth, depth)
         for j, out in enumerate((dq, dk, dv)):
-            out[...] = (yhome[c, :, parts[j]] + yend[1, :, parts[j]].astype(F32)) * 0.125
+            out[...] = (yhome[j, :, here] + yend[j, 1].astype(F32)).T * 0.125
 
     @pl.when(away)
     def _():
         for j, out in enumerate((dq, dk, dv)):
-            out[...] = (yend[0, :, parts[j]].astype(F32) + yend[1, :, parts[j]].astype(F32)) * 0.125
-
-    for cols in (beta, alpha):
+            out[...] = (yend[j, 0].astype(F32) + yend[j, 1].astype(F32)).T * 0.125
+
+    for cols in pieces + (beta,):
         for hf in range(2):
             net.wait(
                 ("d", cols.start), dbuf.at[hf, :, cols], offset=hf, width=2, when=jnp.logical_or(away, c != hf)
@@ -561,6 +616,7 @@
             buf(depth * 8, 3 * columns),
             buf(length, 3 * columns),
             buf(length, 3 * columns),
+            buf(3 * columns, length),
             buf(columns, columns, kind=F32),
             buf(columns, columns, kind=F32),
             buf(2, 8, columns, kind=F32),
@@ -577,14 +633,13 @@
             buf(2, rows, rest),
             buf(2, 2 * rows, rest),
             buf(2, rows, half),
-            buf(2, depth, 3 * columns),
-            buf(2, 2, depth, 3 * columns),
-            buf(2, depth, 3 * columns, kind=F32),
-            buf(2, depth, 3 * columns, kind=F32),
-            buf(2, depth, 3 * columns),
-            buf(2, 2 * depth, 3 * columns),
-            buf(2, depth, 3 * columns),
-            buf(2, depth, 3 * columns),
+            buf(3, columns, 2 * depth),
+            buf(3, 2, columns, 2 * depth),
+            buf(3, columns, 2 * depth, kind=F32),
+            buf(3, 2, columns, depth),
+            buf(3, 2, columns, 2 * depth),
+            buf(3, columns, 2 * depth),
+            buf(3, 2, columns, depth),
             dma((SEMS,)),
             dma((SEMS,)),
         ],

time: 127 us -> 119 us (0.937)
  Pallas kernels: 125 us -> 117 us
    pallas_call x1, Pallas kernels: 124 us -> 116 us  [whole(): pl.pallas_call(whole_kernel, out_shape=(buf(rows, width),) + (buf(depth,...]
where the time goes in v2:
time: 119 us; the launch traced here: 118 us
  Pallas kernels  117 us (98%)
  between operations  1.29 us (1%)
    pallas_call x1, Pallas kernels, whole(): pl.pallas_call(whole_kernel, out_shape=(buf(rows, width),) + (buf(depth,...  116 us

profile of v2, /device:TPU:1, one launch (start us, length us, event | category | flops | bytes accessed | tf_op | source)
XLA Modules:
  0.0 118.5 jit_solution(8730600112188416377)
XLA Ops:
  1.3 116.1 %whole.1 = (bf16[128,2048]{1,0:T(8,128)(2,1)S(1)}, f32[256,256]{1,0:T(8,128)S(1)}, f32[256,256]{1,0:T(8,128)S(1)}, f32[256,256]{1,0:T(8,128)S(1)}) custom-call(f32[1]{0:T(128)S(6)} %copy.10.rate, bf16[128,2048]{1,0:T(8,128)(2,1)} %bitcast.4, bf16[128,4096]{1,0:T(8,128)(2,1)} %bitcast.3, bf16[256,256]{1,0:T(8,128)(2,1)} %wq.1, bf16[256,256]{1,0:T(8,128)(2,1)} %wk.1, ...), custom_call_target="tpu_custom_call" | custom-call | tf_op jit(solution)/shard_map/whole/pallas_call | solution.py:608
  117.4 1.1 finish.1

commit v3 on v2

--- a/solution.py
+++ b/solution.py
@@ -7,7 +7,7 @@
 from jax.experimental.pallas import tpu as pltpu
 from jax.sharding import PartitionSpec as P
 
-BLOCK = 128
+BLOCK = 256
 SIDE = 4
 FIRST = 640
 EARLY = 384
@@ -18,7 +18,10 @@
 NT = (((1,), (1,)), ((), ()))
 TN = (((0,), (0,)), ((), ()))
 VMEM_LIMIT = 60 * 1024 * 1024
-SEMS = 256
+GROUP = 4 * 1024 * 1024
+CELL = 32 * 1024
+SENDS = 9
+RECVS = 125
 
 
 def dot(a, b, dims=NN):
@@ -30,59 +33,67 @@
 
 
 class Net:
-    def __init__(self, send, recv, somewhere):
+    def __init__(self, send, recv, meter, small, somewhere):
         self.send, self.recv, self.somewhere = send, recv, somewhere
-        self.names, self.starts, self.pending = {}, 0, []
+        self.meter, self.small = meter, small
+        self.names, self.total, self.groups, self.open = {}, 0, [], {}
 
     def index(self, name, width=1):
         if name not in self.names:
-            self.names[name] = sum(w for _, w in self.names.values()), width
-        return self.names[name][0]
+            self.names[name] = self.total
+            self.total += width
+        return self.names[name]
+
+    def lane(self, kind, when, size):
+        group = self.open.get(kind)
+        if group is None or self.groups[group][1] + size > GROUP:
+            self.open[kind] = group = len(self.groups)
+            self.groups.append([when, 0])
+        self.groups[group][1] += size
+        return group
+
+    def copy(self, src, dst, lane, slot, where):
+        return pltpu.make_async_remote_copy(
+            src_ref=src, dst_ref=dst, send_sem=self.send.at[lane], recv_sem=self.recv.at[slot],
+            device_id=where, device_id_type=MESH,
+        )
 
     def start(self, name, src, dst, where, offset=0, width=1, when=None):
         slot = self.index(name, width) + offset
-        lane = self.starts
-        self.starts += 1
-
-        def make():
-            return pltpu.make_async_remote_copy(
-                src_ref=src, dst_ref=dst, send_sem=self.send.at[lane], recv_sem=self.recv.at[slot],
-                device_id=where, device_id_type=MESH,
-            )
-
+        size = 2 if src.dtype == BF16 else 4
+        for extent in src.shape:
+            size *= extent
+        lane = self.lane(id(when) if size % CELL == 0 else name, when, size)
         if when is None:
-            make().start()
+            self.copy(src, dst, lane, slot, where).start()
         else:
-            pl.when(when)(lambda: make().start())
-        self.pending.append((when, make))
+            pl.when(when)(lambda: self.copy(src, dst, lane, slot, where).start())
 
     def wait(self, name, dst, offset=0, width=1, when=None):
         slot = self.index(name, width) + offset
-
-        def run():
-            pltpu.make_async_remote_copy(
-                src_ref=dst, dst_ref=dst, send_sem=self.send.at[0], recv_sem=self.recv.at[slot],
-                device_id=self.somewhere, device_id_type=MESH,
-            ).wait_recv()
-
         if when is None:
-            run()
+            self.copy(dst, dst, 0, slot, self.somewhere).wait_recv()
         else:
-            pl.when(when)(run)
+            pl.when(when)(lambda: self.copy(dst, dst, 0, slot, self.somewhere).wait_recv())
 
     def drain(self):
-        for when, make in self.pending:
+        for lane, (when, size) in enumerate(self.groups):
+            ref = self.meter.at[pl.ds(0, size // (2 * self.meter.shape[1]))] if size % CELL == 0 else self.small
+
+            def run():
+                self.copy(ref, ref, lane, 0, self.somewhere).wait_send()
+
             if when is None:
-                make().wait_send()
+                run()
             else:
-                pl.when(when)(lambda make=make: make().wait_send())
+                pl.when(when)(run)
 
 
 def whole_kernel(
-    rate, h_in, c_in, wq, wk, wv, dh, dq, dk, dv,
+    rate, h_far, c_far, wq, wk, wv, dh, dq, dk, dv,
     h_all, c_all, w_all, p_all, g_all, g_turn, state, back, rates, inner, inner_t, decays,
     pout, pin, psum, ra1, ra2, ra3, rb0, rb1, rb2, dbuf,
-    ysend, yone, yhome, yr1, yr2, yout, yend, send, recv,
+    ysend, yone, yhome, yr1, yr2, yout, yend, h_in, c_in, w_in, local, send, recv,
 ):
     s = lax.axis_index("sp")
     d = lax.axis_index("dp")
@@ -113,8 +124,14 @@
     zs = {1: at(zz=turned(z, 1)), -1: at(zz=turned(z, -1))}
     ys = {1: at(yy=turned(y, 1)), -1: at(yy=turned(y, -1))}
     cross = 3 - x
-    net = Net(send, recv, mate)
-    weights = (wq, wk, wv)
+    net = Net(send, recv, h_all, rates.at[0], mate)
+    weights = [w_in.at[j] for j in range(3)]
+    loads = [
+        pltpu.make_async_copy(src, dst, local.at[i])
+        for i, (src, dst) in enumerate(zip((h_far, wq, wk, wv, c_far), [h_in] + weights + [c_in]))
+    ]
+    for load in loads:
+        load.start()
 
     barrier = pltpu.get_barrier_semaphore()
     peers = [mate, ys[1], ys[-1]]
@@ -124,7 +141,11 @@
     for where in peers:
         pl.semaphore_signal(barrier, inc=1, device_id=where, device_id_type=MESH)
     rates[0] = jnp.full(rates.shape[1:], rate[0], F32)
+    loads[0].wait()
     pl.semaphore_wait(barrier, len(peers))
+
+    def r_rows(r):
+        return span(turned(z, r) * four, four, four)
 
     def slot(r, col, b):
         return turned(z, r) * SIDE + 2 * (xl if col == 0 else 1 - xl) + b
@@ -139,7 +160,7 @@
         net.start(name, ref, ref, where)
 
     def to_mate(r, col, b, part):
-        h_send(r, col, b, part, mate, ("m", r, col, b, part))
+        h_send(r, col, b, part, mate, ("m", r))
 
     def h_wait(r, col, b, part, when=None):
         net.wait(("x", r, col, b, part), h_ref(slot(r, col, b), part, c), when=when)
@@ -162,6 +183,8 @@
             ("x", 0, 0, 1, "f"), h_in.at[:, pl.ds(hf * half, half)], h_ref(there, "f", hf),
             at(xx=cross, cc=hf), when=away,
         )
+    for load in loads[1:4]:
+        load.wait()
     for j in range(3):
         w_near(j)
     for j in range(3):
@@ -220,6 +243,19 @@
         h_wait(2, 0, b, "f")
         h_send(2, 0, b, "b", pair, ("x", 2, 1, b, "b"))
         to_mate(2, 0, b, "f")
+
+    def c_send(dz, dx):
+        hz, hx = turned(z, dz), turned(x, dx)
+        head = hz * SIDE + hx
+        far = (hx // 2 - c) * (hx // 2 - c)
+        net.start(
+            ("c",), c_in.at[:, span(head * columns, columns, columns)],
+            c_all.at[span(s * rows, rows, rows)],
+            {"sp": hz * SIDE + hx + far * (3 - 2 * hx), "dp": y * 2 + c + far * (1 - 2 * c)},
+            offset=s, width=blocks, when=away if (dz, dx) == (0, 0) else None,
+        )
+
+    diagonal = [(dz, (dz + k) % SIDE) for k in range(SIDE) for dz in (2, 1, 3, 0)]
 
     h_wait(0, 0, 0, "f", when=away)
     spread(0)
@@ -239,6 +275,14 @@
     w_spread(1, away)
     w_forward(2, own)
     w_spread(2, away)
+    loads[4].wait()
+    for dz, dx in diagonal[:8]:
+        c_send(dz, dx)
+
+    @pl.when(own)
+    def _():
+        c_all[span(s * rows, rows, rows), :] = c_in[:, span(s * columns, columns, columns)]
+
     from_far(0)
     from_corner(0)
     w_forward(0, away)
@@ -246,69 +290,44 @@
     from_corner(1)
     w_forward(1, away)
 
-    def c_send(hop, when=None):
-        head = (s + hop) % blocks
-        hz, hx = head // SIDE, head % SIDE
-        far = (hx // 2 - c) * (hx // 2 - c)
-        net.start(
-            ("c",), c_in.at[:, span(head * columns, columns, columns)],
-            c_all.at[span(s * rows, rows, rows)],
-            {"sp": hz * SIDE + hx + far * (3 - 2 * hx), "dp": y * 2 + c + far * (1 - 2 * c)},
-            offset=s, width=blocks, when=when,
-        )
-
-    c_send(0, when=away)
-    for hop in range(1, blocks):
-        c_send(hop)
-
-    @pl.when(own)
-    def _():
-        c_all[span(s * rows, rows, rows), :] = c_in[:, span(s * columns, columns, columns)]
+    for dz, dx in diagonal[8:]:
+        c_send(dz, dx)
 
     for r in (-1, 1):
         for b in range(2):
             h_wait(r, 1, b, "b")
             to_mate(r, 1, b, "b")
     w_forward(2, away)
-    for b in range(2):
-        h_wait(2, 1, b, "a")
-        to_mate(2, 1, b, "a")
-    for b in range(2):
-        h_wait(2, 1, b, "b")
-        to_mate(2, 1, b, "b")
+
+    def mate_wait(r):
+        net.wait(("m", r), h_all.at[r_rows(r), theirs])
+
+    def project(first, step, count):
+        @pl.loop(0, 3 * count)
+        def _(t):
+            place = span(turned(z, first + step * (t // 3)) * four, four, four)
+            j = t % 3
+            cols = span(j * columns, columns, columns)
+            value = dot(h_all[place, :], w_all[:, cols]).astype(BF16)
+            factor = jnp.where(j == 1, scale, 1.0).astype(F32)
+            p_all[place, cols] = (value.astype(F32) * factor).astype(BF16)
 
     for j in range(3):
         for way, cc in ((1, 1), (-1, 0)):
             net.wait(("w1", j, -way, cc), w_ref(turned(y, -way), cc, j))
         for cc in range(2):
             net.wait(("w2", j, cc), w_ref(turned(y, 2), cc, j))
-
-    def mate_wait(r):
-        for col in range(2):
-            for b in range(2):
-                for part in ("f",) if col == 0 or r == 0 else ("a", "b"):
-                    net.wait(("m", r, col, b, part), h_ref(slot(r, col, b), part, 1 - c))
-
-    def project(r, j):
-        place = span(turned(z, r) * four, four, four)
-        cols = span(j * columns, columns, columns)
-        value = dot(h_all[place, :], w_all[:, cols]).astype(BF16)
-        factor = jnp.where(j == 1, scale, 1.0).astype(F32)
-        p_all[place, cols] = (value.astype(F32) * factor).astype(BF16)
-
-    for r in (0, 1, -1):
-        mate_wait(r)
-
-    @pl.loop(0, 9)
-    def _(t):
-        o = t // 3
-        project(o + o // 2, t % 3)
-
+    mate_wait(0)
+    project(0, 0, 1)
+    for part in ("a", "b"):
+        for b in range(2):
+            h_wait(2, 1, b, part)
+            to_mate(2, 1, b, part)
+    mate_wait(1)
+    mate_wait(-1)
+    project(1, 2, 2)
     mate_wait(2)
-
-    @pl.loop(0, 3)
-    def _(j):
-        project(2, j)
+    project(2, 0, 1)
 
     net.wait(("rate",), rates.at[1])
     for k in range(blocks):
@@ -325,38 +344,50 @@
         lax.broadcasted_iota(jnp.int32, (BLOCK, BLOCK), 0) - lax.broadcasted_iota(jnp.int32, (BLOCK, BLOCK), 1)
     ).astype(F32)
     place = lax.broadcasted_iota(jnp.int32, (BLOCK, columns), 0).astype(F32)
-    g_sq = g_row[:, :BLOCK]
-    inner[...] = jnp.where(gap >= 0, jnp.exp(g_sq * jnp.maximum(gap, 0.0)), 0.0)
-    inner_t[...] = jnp.where(gap <= 0, jnp.exp(g_sq * jnp.maximum(-gap, 0.0)), 0.0)
+    inner[...] = jnp.where(gap >= 0, jnp.exp(g_row * jnp.maximum(gap, 0.0)), 0.0)
+    inner_t[...] = jnp.where(gap <= 0, jnp.exp(g_row * jnp.maximum(-gap, 0.0)), 0.0)
     decays[0] = jnp.exp(g_row * (place + 1.0))
     decays[1] = jnp.exp(g_row * (BLOCK - 1.0 - place))
     block_decay = jnp.exp(g_row * BLOCK)
     state[...] = jnp.zeros_like(state)
     back[...] = jnp.zeros_like(back)
     parts = [slice(j * columns, (j + 1) * columns) for j in range(3)]
-
-    def slot_of(i):
-        iz, ix = i // SIDE, i % SIDE
-        b = (ix // 2 - u) * (ix // 2 - u)
-        return iz * SIDE + 2 * (ix + b * (3 - 2 * ix) - 2 * u) + b
-
-    @pl.loop(0, blocks)
-    def _(i):
-        put = span(slot_of(i) * BLOCK, BLOCK, BLOCK)
-        k, v = p_all[put, parts[1]], p_all[put, parts[2]]
+    count = BLOCK // rows
+
+    def slots(i):
+        places = []
+        for w in range(count):
+            p = i * count + w
+            pz, px = p // SIDE, p % SIDE
+            b = (px // 2 - u) * (px // 2 - u)
+            places.append(span((pz * SIDE + 2 * (px + b * (3 - 2 * px) - 2 * u) + b) * rows, rows, rows))
+        return places
+
+    def get(places, part):
+        return jnp.concatenate([p_all[place, part] for place in places], axis=0)
+
+    def put(places, part, grad):
+        grad = grad.astype(BF16)
+        for w, place in enumerate(places):
+            g_all[place, part] = grad[w * rows : (w + 1) * rows]
+        grad = grad.T
+        for w, place in enumerate(places):
+            g_turn[part, place] = grad[:, w * rows : (w + 1) * rows]
+
+    def forward(i):
+        places = slots(i)
+        k, v = get(places, parts[1]), get(places, parts[2])
         ct = c_all[span(i * BLOCK, BLOCK, BLOCK), :]
         mixed = (dot(ct, v, NT) * inner[...]).astype(BF16)
         held = state[...]
         grad_q = dot(mixed, k) + dot(ct, held.astype(BF16), NT) * decays[0]
         weighted = (k.astype(F32) * decays[1]).astype(BF16)
         state[...] = held * block_decay + dot(weighted, v, TN)
-        grad_q = grad_q.astype(BF16)
-        g_all[put, parts[0]] = grad_q
-        g_turn[parts[0], put] = grad_q.T
-
-        i = blocks - 1 - i
-        put = span(slot_of(i) * BLOCK, BLOCK, BLOCK)
-        q, k, v = (p_all[put, part] for part in parts)
+        put(places, parts[0], grad_q)
+
+    def backward(i):
+        places = slots(i)
+        q, k, v = (get(places, part) for part in parts)
         ct = c_all[span(i * BLOCK, BLOCK, BLOCK), :]
         mixed_t = (dot(v, ct, NT) * inner_t[...]).astype(BF16)
         scores_t = (dot(k, q, NT) * inner_t[...]).astype(BF16)
@@ -366,16 +397,20 @@
         grad_k = (dot(mixed_t, q) + dot(v, held_bf, NT) * decays[1]) * scale
         weighted = (q.astype(F32) * decays[0]).astype(BF16)
         back[...] = held * block_decay + dot(weighted, ct, TN)
-        for part, grad in ((parts[1], grad_k.astype(BF16)), (parts[2], grad_v.astype(BF16))):
-            g_all[put, part] = grad
-            g_turn[part, put] = grad.T
+        put(places, parts[1], grad_k)
+        put(places, parts[2], grad_v)
+
+    steps = rows * blocks // BLOCK
+
+    @pl.loop(0, steps // 2)
+    def _(t):
+        for w in range(2):
+            forward(2 * t + w)
+            backward(steps - 1 - 2 * t - w)
 
     pieces = (pl.ds(0, EARLY), pl.ds(EARLY, FIRST - EARLY))
     beta = pl.ds(FIRST, half - FIRST)
     chunk = half // 2
-
-    def r_rows(r):
-        return span(turned(z, r) * four, four, four)
 
     def pick_rows(r, hf):
         return span(turned(z, r) * four + hf * two, two, two)
@@ -590,6 +625,7 @@
     for hf in range(2):
         dh[:, hf * half : (hf + 1) * half] = dbuf[hf]
     net.drain()
+    assert len(net.groups) <= SENDS and net.total <= RECVS, (len(net.groups), net.total)
 
 
 def whole(rate, h, c, wq, wk, wv):
@@ -608,7 +644,7 @@
     return pl.pallas_call(
         whole_kernel,
         out_shape=(buf(rows, width),) + (buf(depth, columns, kind=F32),) * 3,
-        in_specs=[pl.BlockSpec(memory_space=pltpu.SMEM)] + [vmem] * 5,
+        in_specs=[pl.BlockSpec(memory_space=pltpu.SMEM)] + [pl.BlockSpec(memory_space=pl.ANY)] * 5,
         out_specs=(vmem,) * 4,
         scratch_shapes=[
             buf(length, width),
@@ -640,8 +676,12 @@
             buf(3, 2, columns, 2 * depth),
             buf(3, columns, 2 * depth),
             buf(3, 2, columns, depth),
-            dma((SEMS,)),
-            dma((SEMS,)),
+            buf(rows, width),
+            buf(rows, columns * blocks),
+            buf(3, depth, columns),
+            dma((5,)),
+            dma((SENDS,)),
+            dma((RECVS,)),
         ],
         compiler_params=pltpu.CompilerParams(
             collective_id=0, has_side_effects=True, vmem_limit_bytes=VMEM_LIMIT

time: 119 us -> 108 us (0.908)
  Pallas kernels: 117 us -> 107 us
    pallas_call x1, Pallas kernels: 116 us -> 106 us  [whole(): pl.pallas_call(whole_kernel, out_shape=(buf(rows, width),) + (buf(depth,...]
where the time goes in v3:
time: 108 us
  Pallas kernels  107 us (99%)
  between operations  1.45 us (1%)
    pallas_call x1, Pallas kernels, whole(): pl.pallas_call(whole_kernel, out_shape=(buf(rows, width),) + (buf(depth,...  106 us

profile of v3, /device:TPU:1, one launch (start us, length us, event | category | flops | bytes accessed | tf_op | source)
XLA Modules:
  0.0 108.1 jit_solution(16787323308419863389)
XLA Ops:
  1.3 105.6 %whole.1 = (bf16[128,2048]{1,0:T(8,128)(2,1)S(1)}, f32[256,256]{1,0:T(8,128)S(1)}, f32[256,256]{1,0:T(8,128)S(1)}, f32[256,256]{1,0:T(8,128)S(1)}) custom-call(f32[1]{0:T(128)S(6)} %copy.10.rate, bf16[128,2048]{1,0:T(8,128)(2,1)} %bitcast.4, bf16[128,4096]{1,0:T(8,128)(2,1)} %bitcast.3, bf16[256,256]{1,0:T(8,128)(2,1)} %wq.1, bf16[256,256]{1,0:T(8,128)(2,1)} %wk.1, ...), custom_call_target="tpu_custom_call" | custom-call | tf_op jit(solution)/shard_map/whole/pallas_call | solution.py:644
  106.9 1.1 %finish.1 = (bf16[128,2048]{1,0:T(8,128)(2,1)}, f32[256,256]{1,0:T(8,128)}, f32[256,256]{1,0:T(8,128)}, f32[256,256]{1,0:T(8,128)}) custom-call(bf16[128,2048]{1,0:T(8,128)(2,1)S(1)} %get-tuple-element.12.refs_0_, f32[256,256]{1,0:T(8,128)S(1)} %get-tuple-element.13.refs_1_, f32[256,256]{1,0:T(8,128)S(1)} %get-tuple-element.14.refs_2_, ...), custom_call_target="tpu_custom_call" | custom-call | tf_op jit(solution)/shard_map/finish/pallas_call | solution.py:704

commit v4 on v3

--- a/solution.py
+++ b/solution.py
@@ -21,7 +21,7 @@
 GROUP = 4 * 1024 * 1024
 CELL = 32 * 1024
 SENDS = 9
-RECVS = 125
+RECVS = 120
 
 
 def dot(a, b, dims=NN):
@@ -208,13 +208,14 @@
             far = who if who is away else jnp.logical_and(own, c != cc)
             net.wait(("w0", j), w_ref(y, cc, j), offset=cc, width=2, when=far)
             for way in (1, -1):
-                net.start(("w1", j, -way, cc), w_ref(y, cc, j), w_ref(y, cc, j), ys[way], when=who)
+                name = ("w1", j, -way) if (way == 1) == (cc == 0) else ("wt", j)
+                net.start(name, w_ref(y, cc, j), w_ref(y, cc, j), ys[way], when=who)
 
     def w_forward(j, who):
         for way, cc in ((1, 0), (-1, 1)):
             ref = w_ref(turned(y, -way), cc, j)
-            net.wait(("w1", j, -way, cc), ref, when=who)
-            net.start(("w2", j, cc), ref, ref, ys[way], when=who)
+            net.wait(("w1", j, -way), ref, when=who)
+            net.start(("wt", j), ref, ref, ys[way], when=who)
 
     def from_pair(b):
         h_wait(0, 1, b, "f")
@@ -283,21 +284,9 @@
     def _():
         c_all[span(s * rows, rows, rows), :] = c_in[:, span(s * columns, columns, columns)]
 
-    from_far(0)
-    from_corner(0)
-    w_forward(0, away)
-    from_far(1)
-    from_corner(1)
-    w_forward(1, away)
-
-    for dz, dx in diagonal[8:]:
-        c_send(dz, dx)
-
-    for r in (-1, 1):
-        for b in range(2):
-            h_wait(r, 1, b, "b")
-            to_mate(r, 1, b, "b")
-    w_forward(2, away)
+    def w_ready(who):
+        for j in range(3):
+            net.wait(("wt", j), w_all.at[pl.ds(0, 4 * depth), pl.ds(j * columns, columns)], when=who)
 
     def mate_wait(r):
         net.wait(("m", r), h_all.at[r_rows(r), theirs])
@@ -312,13 +301,27 @@
             factor = jnp.where(j == 1, scale, 1.0).astype(F32)
             p_all[place, cols] = (value.astype(F32) * factor).astype(BF16)
 
-    for j in range(3):
-        for way, cc in ((1, 1), (-1, 0)):
-            net.wait(("w1", j, -way, cc), w_ref(turned(y, -way), cc, j))
-        for cc in range(2):
-            net.wait(("w2", j, cc), w_ref(turned(y, 2), cc, j))
+    def betas(b):
+        for r in (-1, 1):
+            h_wait(r, 1, b, "b")
+            to_mate(r, 1, b, "b")
+
+    from_far(0)
+    betas(0)
+    w_forward(0, away)
+    w_forward(1, away)
     mate_wait(0)
-    project(0, 0, 1)
+    w_ready(own)
+    pl.when(own)(lambda: project(0, 0, 1))
+    w_forward(2, away)
+    from_corner(0)
+    betas(1)
+    from_far(1)
+    from_corner(1)
+    for dz, dx in diagonal[8:]:
+        c_send(dz, dx)
+    w_ready(away)
+    pl.when(away)(lambda: project(0, 0, 1))
     for part in ("a", "b"):
         for b in range(2):
             h_wait(2, 1, b, part)
@@ -415,27 +418,19 @@
     def pick_rows(r, hf):
         return span(turned(z, r) * four + hf * two, two, two)
 
-    def other(r):
-        lhs_rows = r_rows(r)
-
-        @pl.loop(0, 2)
-        def _(i):
-            value = dot(g_all[lhs_rows, :], w_all[span((1 - c) * half + i * chunk, chunk, chunk), :], NT)
-            pout[lhs_rows, span(i * chunk, chunk, chunk)] = value.astype(BF16)
-
-        net.start(("p", r), pout.at[lhs_rows], pin.at[lhs_rows], mate)
-
-    def summed(r):
-        lhs_rows = r_rows(r)
-        net.wait(("p", r), pin.at[lhs_rows])
-
-        @pl.loop(0, 2)
-        def _(i):
-            value = dot(g_all[lhs_rows, :], w_all[span(c * half + i * chunk, chunk, chunk), :], NT)
-            cols = span(i * chunk, chunk, chunk)
-            psum[lhs_rows, cols] = (value + pin[lhs_rows, cols].astype(F32)).astype(BF16)
-
-        net.start(("b0", r), psum.at[pick_rows(r, 1 - xl), beta], rb0.at[r % SIDE], pair)
+    def other(r, i):
+        cols = span(i * chunk, chunk, chunk)
+        value = dot(g_all[r_rows(r), :], w_all[span((1 - c) * half + i * chunk, chunk, chunk), :], NT)
+        pout[r_rows(r), cols] = value.astype(BF16)
+        net.start(("p", r, i), pout.at[r_rows(r), cols], pin.at[r_rows(r), cols], mate)
+
+    def summed(r, i):
+        cols = span(i * chunk, chunk, chunk)
+        net.wait(("p", r, i), pin.at[r_rows(r), cols])
+        value = dot(g_all[r_rows(r), :], w_all[span(c * half + i * chunk, chunk, chunk), :], NT)
+        psum[r_rows(r), cols] = (value + pin[r_rows(r), cols].astype(F32)).astype(BF16)
+        if i == 1:
+            net.start(("b0", r), psum.at[pick_rows(r, 1 - xl), beta], rb0.at[r % SIDE], pair)
 
     def add(place, cols, *refs):
         total = psum[place, cols].astype(F32)
@@ -561,28 +556,36 @@
         for hf in range(2):
             net.start(("e", j, 1), yout.at[j, :, lanes[hf]], yend.at[j, 1], at(xx=cross, cc=hf), when=away)
 
-    other(2)
     y_first(0)
+    other(2, 0)
+    other(2, 1)
     y_first(1)
-    summed(2)
+    summed(2, 0)
     alpha_first(0)
+    summed(2, 1)
     alpha_first(1)
-    other(1)
     y_first(2)
-    other(-1)
-    summed(1)
+    other(1, 0)
+    other(1, 1)
+    other(-1, 0)
+    other(-1, 1)
+    y_second(0)
+    summed(1, 0)
     alpha_plain(0, 1)
-    summed(-1)
+    summed(-1, 0)
     alpha_plain(0, -1)
-    y_second(0)
+    summed(1, 1)
+    summed(-1, 1)
     alpha_added(0)
     alpha_plain(1, 1)
     alpha_plain(1, -1)
-    other(0)
     y_second(1)
+    other(0, 0)
+    other(0, 1)
     alpha_added(1)
     beta_first()
-    summed(0)
+    summed(0, 0)
+    summed(0, 1)
     y_second(2)
     beta_plain()
     for j in range(3):

time: 108 us -> 102 us (0.944)
  Pallas kernels: 107 us -> 101 us
    pallas_call x1, Pallas kernels: 106 us -> 99.5 us  [whole(): pl.pallas_call(whole_kernel, out_shape=(buf(rows, width),) + (buf(depth,...]
where the time goes in v4:
time: 102 us
  Pallas kernels  101 us (99%)
  between operations  1.45 us (1%)
    pallas_call x1, Pallas kernels, whole(): pl.pallas_call(whole_kernel, out_shape=(buf(rows, width),) + (buf(depth,...  99.5 us

profile of v4, /device:TPU:1, one launch (start us, length us, event | category | flops | bytes accessed | tf_op | source)
XLA Modules:
  0.0 102.0 jit_solution(2564401510216153801)
XLA Ops:
  1.3 99.5 %whole.1 = (bf16[128,2048]{1,0:T(8,128)(2,1)S(1)}, f32[256,256]{1,0:T(8,128)S(1)}, f32[256,256]{1,0:T(8,128)S(1)}, f32[256,256]{1,0:T(8,128)S(1)}) custom-call(f32[1]{0:T(128)S(6)} %copy.10.rate, bf16[128,2048]{1,0:T(8,128)(2,1)} %bitcast.4, bf16[128,4096]{1,0:T(8,128)(2,1)} %bitcast.3, bf16[256,256]{1,0:T(8,128)(2,1)} %wq.1, bf16[256,256]{1,0:T(8,128)(2,1)} %wk.1, ...), custom_call_target="tpu_custom_call" | custom-call | tf_op jit(solution)/shard_map/whole/pallas_call | solution.py:647
  100.8 1.1 %finish.1 = (bf16[128,2048]{1,0:T(8,128)(2,1)}, f32[256,256]{1,0:T(8,128)}, f32[256,256]{1,0:T(8,128)}, f32[256,256]{1,0:T(8,128)}) custom-call(bf16[128,2048]{1,0:T(8,128)(2,1)S(1)} %get-tuple-element.12.refs_0_, f32[256,256]{1,0:T(8,128)S(1)} %get-tuple-element.13.refs_1_, f32[256,256]{1,0:T(8,128)S(1)} %get-tuple-element.14.refs_2_, ...), custom_call_target="tpu_custom_call" | custom-call | tf_op jit(solution)/shard_map/finish/pallas_call | solution.py:707

commit v5 on v4

--- a/solution.py
+++ b/solution.py
@@ -10,7 +10,8 @@
 BLOCK = 256
 SIDE = 4
 FIRST = 640
-EARLY = 384
+PIECES = ((512, 128), (0, 256), (256, 256))
+EAGER = 12
 F32 = jnp.float32
 BF16 = jnp.bfloat16
 MESH = pl.DeviceIdType.MESH
@@ -21,7 +22,7 @@
 GROUP = 4 * 1024 * 1024
 CELL = 32 * 1024
 SENDS = 9
-RECVS = 120
+RECVS = 83
 
 
 def dot(a, b, dims=NN):
@@ -224,13 +225,14 @@
         to_mate(0, 1, b, "f")
 
     def from_side(b):
-        fast = 1 if b == 0 else -1
-        for r in (-fast, fast):
+        for r in (-1, 1):
             h_wait(r, 0, b, "f")
-            if r == -fast:
-                h_send(r, 0, b, "f", zs[fast], ("x", 2, 0, b, "f"))
             h_send(r, 0, b, "b", pair, ("x", r, 1, b, "b"))
             to_mate(r, 0, b, "f")
+
+    def side_forward(b):
+        fast = 1 if b == 0 else -1
+        h_send(-fast, 0, b, "f", zs[fast], ("x", 2, 0, b, "f"))
 
     def from_corner(b):
         fast = 1 if b == 0 else -1
@@ -253,7 +255,7 @@
             ("c",), c_in.at[:, span(head * columns, columns, columns)],
             c_all.at[span(s * rows, rows, rows)],
             {"sp": hz * SIDE + hx + far * (3 - 2 * hx), "dp": y * 2 + c + far * (1 - 2 * c)},
-            offset=s, width=blocks, when=away if (dz, dx) == (0, 0) else None,
+            when=away if (dz, dx) == (0, 0) else None,
         )
 
     diagonal = [(dz, (dz + k) % SIDE) for k in range(SIDE) for dz in (2, 1, 3, 0)]
@@ -272,73 +274,78 @@
     w_spread(0, away)
     from_side(1)
     from_pair(1)
+    side_forward(0)
+    side_forward(1)
     w_forward(1, own)
     w_spread(1, away)
     w_forward(2, own)
     w_spread(2, away)
-    loads[4].wait()
-    for dz, dx in diagonal[:8]:
-        c_send(dz, dx)
-
-    @pl.when(own)
-    def _():
-        c_all[span(s * rows, rows, rows), :] = c_in[:, span(s * columns, columns, columns)]
-
-    def w_ready(who):
-        for j in range(3):
-            net.wait(("wt", j), w_all.at[pl.ds(0, 4 * depth), pl.ds(j * columns, columns)], when=who)
+
+    def w_ready(j):
+        net.wait(("wt", j), w_all.at[pl.ds(0, 4 * depth), pl.ds(j * columns, columns)])
 
     def mate_wait(r):
         net.wait(("m", r), h_all.at[r_rows(r), theirs])
 
-    def project(first, step, count):
-        @pl.loop(0, 3 * count)
+    def project(row, j):
+        place = span(row * four, four, four)
+        cols = span(j * columns, columns, columns)
+        value = dot(h_all[place, :], w_all[:, cols]).astype(BF16)
+        factor = jnp.where(j == 1, scale, 1.0).astype(F32)
+        p_all[place, cols] = (value.astype(F32) * factor).astype(BF16)
+
+    def project_near(j):
+        @pl.loop(0, 3)
         def _(t):
-            place = span(turned(z, first + step * (t // 3)) * four, four, four)
-            j = t % 3
-            cols = span(j * columns, columns, columns)
-            value = dot(h_all[place, :], w_all[:, cols]).astype(BF16)
-            factor = jnp.where(j == 1, scale, 1.0).astype(F32)
-            p_all[place, cols] = (value.astype(F32) * factor).astype(BF16)
+            project(turned(z, t + t // 2), j)
 
     def betas(b):
         for r in (-1, 1):
             h_wait(r, 1, b, "b")
             to_mate(r, 1, b, "b")
 
-    from_far(0)
-    betas(0)
-    w_forward(0, away)
-    w_forward(1, away)
-    mate_wait(0)
-    w_ready(own)
-    pl.when(own)(lambda: project(0, 0, 1))
-    w_forward(2, away)
-    from_corner(0)
-    betas(1)
-    from_far(1)
-    from_corner(1)
-    for dz, dx in diagonal[8:]:
-        c_send(dz, dx)
-    w_ready(away)
-    pl.when(away)(lambda: project(0, 0, 1))
-    for part in ("a", "b"):
+    def fars(part):
         for b in range(2):
             h_wait(2, 1, b, part)
             to_mate(2, 1, b, part)
-    mate_wait(1)
-    mate_wait(-1)
-    project(1, 2, 2)
+
+    from_corner(0)
+    betas(0)
+    w_forward(0, away)
+    from_corner(1)
+    loads[4].wait()
+    for dz, dx in diagonal[:EAGER]:
+        c_send(dz, dx)
+    betas(1)
+    w_forward(1, away)
+    w_forward(2, away)
+    for r in (0, 1, -1):
+        mate_wait(r)
+    w_ready(0)
+    project_near(0)
+    from_far(0)
+    from_far(1)
+    for dz, dx in diagonal[EAGER:]:
+        c_send(dz, dx)
+
+    @pl.when(own)
+    def _():
+        c_all[span(s * rows, rows, rows), :] = c_in[:, span(s * columns, columns, columns)]
+
+    w_ready(1)
+    project_near(1)
+    w_ready(2)
+    project_near(2)
+    fars("a")
+    fars("b")
     mate_wait(2)
-    project(2, 0, 1)
+    @pl.loop(0, 3)
+    def _(j):
+        project(turned(z, 2), j)
 
     net.wait(("rate",), rates.at[1])
-    for k in range(blocks):
-        source = (s + k) % blocks
-        net.wait(
-            ("c",), c_all.at[span(source * rows, rows, rows)], offset=source, width=blocks,
-            when=away if k == 0 else None,
-        )
+    for who, taken in ((own, blocks - 1), (away, blocks)):
+        net.wait(("c",), c_all.at[pl.ds(0, taken * rows)], when=who)
 
     pick = jnp.where(own, 1.0, 0.0).astype(F32)
     g = rates[0] * pick + rates[1] * (1.0 - pick)
@@ -411,7 +418,7 @@
             forward(2 * t + w)
             backward(steps - 1 - 2 * t - w)
 
-    pieces = (pl.ds(0, EARLY), pl.ds(EARLY, FIRST - EARLY))
+    pieces = tuple(pl.ds(first, size) for first, size in PIECES)
     beta = pl.ds(FIRST, half - FIRST)
     chunk = half // 2
 
@@ -456,26 +463,24 @@
 
     def alpha_plain(i, r):
         e = 0 if r == 1 else 1
-        alpha_send(i, r, 1 - e, r, ("a2", i, e, 1 - e), a2(i, e, 1 - e))
+        alpha_send(i, r, 1 - e, r, ("a2", i), a2(i, e, 1 - e))
 
     def alpha_added(i):
         for e, r in ((0, 1), (1, -1)):
             net.wait(("a1", i, e), a1(i, e))
             add(pick_rows(r, e), pieces[i], a1(i, e)[...])
-            alpha_send(i, r, e, r, ("a2", i, e, e), a2(i, e, e))
+            alpha_send(i, r, e, r, ("a2", i), a2(i, e, e))
 
     def alpha_last(i):
-        for e, hf in ((0, 1), (1, 0), (0, 0), (1, 1)):
-            net.wait(("a2", i, e, hf), a2(i, e, hf))
+        net.wait(("a2", i), ra2.at[:, :, pieces[i]])
         for hf in range(2):
             add(pick_rows(0, hf), pieces[i], a2(i, 0, hf)[...], a2(i, 1, hf)[...])
         net.start(("a3", i), psum.at[pick_rows(0, 1 - xl), pieces[i]], a3(i), pair)
 
     def deliver(cols):
-        lo = cols.start
         dst = dbuf.at[c, :, cols]
-        net.start(("d", lo), psum.at[b_rows(0, 1), cols], dst, at(xx=cross, cc=u), offset=c, width=2)
-        net.start(("d", lo), psum.at[b_rows(0, 0), cols], dst, mate, offset=c, width=2, when=away)
+        net.start(("d",), psum.at[b_rows(0, 1), cols], dst, at(xx=cross, cc=u), offset=c, width=2)
+        net.start(("d",), psum.at[b_rows(0, 0), cols], dst, mate, offset=c, width=2, when=away)
 
     def alpha_deliver(i):
         net.wait(("a3", i), a3(i))
@@ -503,18 +508,17 @@
     def beta_plain():
         for r, b, e in ((1, 1, 0), (-1, 0, 1)):
             beta_take(r)
-            beta_send(r, b, r, ("b2", e, b), b2(e, b))
+            beta_send(r, b, r, ("b2",), b2(e, b))
 
     def beta_added():
         for r, b, e in ((1, 0, 0), (-1, 1, 1)):
             net.wait(("b1", e), rb1.at[e])
             add(b_rows(r, b), beta, rb1[e])
-            beta_send(r, b, r, ("b2", e, b), b2(e, b))
+            beta_send(r, b, r, ("b2",), b2(e, b))
 
     def beta_last():
         beta_take(0)
-        for e, b in ((0, 1), (1, 0), (0, 0), (1, 1)):
-            net.wait(("b2", e, b), b2(e, b))
+        net.wait(("b2",), rb2)
         add(pick_rows(0, xl), beta, rb2[0], rb2[1])
         deliver(beta)
 
@@ -537,72 +541,77 @@
             value = w_grad(r, j)
             keep = value[:, e * depth : (e + 1) * depth]
             yone[j, e, :, lanes[1 - e]] = value[:, (1 - e) * depth : (2 - e) * depth].astype(BF16)
-            net.start(("y2", j, e, 1 - e), yone.at[j, e, :, lanes[1 - e]], y2(j, e, 1 - e), ys[r])
+            net.start(("y2", j), yone.at[j, e, :, lanes[1 - e]], y2(j, e, 1 - e), ys[r])
             net.wait(("y1", j, e), yr1.at[j, e])
             yone[j, e, :, lanes[e]] = (keep + yr1[j, e].astype(F32)).astype(BF16)
-            net.start(("y2", j, e, e), yone.at[j, e, :, lanes[e]], y2(j, e, e), ys[r])
+            net.start(("y2", j), yone.at[j, e, :, lanes[e]], y2(j, e, e), ys[r])
 
     def y_home(j):
         yhome[j] = w_grad(0, j)
 
     def y_last(j):
-        for e, hf in ((0, 1), (1, 0), (0, 0), (1, 1)):
-            net.wait(("y2", j, e, hf), y2(j, e, hf))
+        net.wait(("y2", j), yr2.at[j])
         total = yhome[j] + yr2[j, 0].astype(F32) + yr2[j, 1].astype(F32)
         yhome[j] = total
         yout[j] = total.astype(BF16)
         half_of = span((1 - c) * depth, depth, depth)
-        net.start(("e", j, 0), yout.at[j, :, half_of], yend.at[j, 0], mate, when=own)
+        net.start(("e", 0), yout.at[j, :, half_of], yend.at[j, 0], mate, when=own)
         for hf in range(2):
-            net.start(("e", j, 1), yout.at[j, :, lanes[hf]], yend.at[j, 1], at(xx=cross, cc=hf), when=away)
+            net.start(("e", 1), yout.at[j, :, lanes[hf]], yend.at[j, 1], at(xx=cross, cc=hf), when=away)
 
     y_first(0)
+    other(2, 1)
     other(2, 0)
-    other(2, 1)
     y_first(1)
+    summed(2, 1)
+    alpha_first(0)
     summed(2, 0)
-    alpha_first(0)
-    summed(2, 1)
     alpha_first(1)
+    alpha_first(2)
     y_first(2)
+    other(1, 1)
+    other(-1, 1)
     other(1, 0)
-    other(1, 1)
     other(-1, 0)
-    other(-1, 1)
     y_second(0)
+    summed(1, 1)
+    alpha_plain(0, 1)
+    summed(-1, 1)
+    alpha_plain(0, -1)
     summed(1, 0)
-    alpha_plain(0, 1)
+    alpha_plain(1, 1)
     summed(-1, 0)
-    alpha_plain(0, -1)
-    summed(1, 1)
-    summed(-1, 1)
+    alpha_plain(1, -1)
+    beta_first()
     alpha_added(0)
-    alpha_plain(1, 1)
-    alpha_plain(1, -1)
     y_second(1)
+    other(0, 1)
     other(0, 0)
-    other(0, 1)
     alpha_added(1)
-    beta_first()
+    alpha_plain(2, 1)
+    alpha_plain(2, -1)
+    alpha_added(2)
+    y_second(2)
+    summed(0, 1)
     summed(0, 0)
-    summed(0, 1)
-    y_second(2)
+    y_home(0)
+    y_last(0)
+    y_home(1)
+    y_home(2)
     beta_plain()
-    for j in range(3):
-        y_home(j)
-    y_last(0)
     alpha_last(0)
     y_last(1)
     alpha_last(1)
+    beta_added()
     alpha_deliver(0)
-    beta_added()
+    alpha_last(2)
+    alpha_deliver(1)
     y_last(2)
-    alpha_deliver(1)
     beta_last()
-
-    for j in range(3):
-        net.wait(("e", j, 1), yend.at[j, 1])
-        net.wait(("e", j, 0), yend.at[j, 0], when=away)
+    alpha_deliver(2)
+
+    net.wait(("e", 1), yend.at[:, 1])
+    net.wait(("e", 0), yend.at[:, 0], when=away)
 
     @pl.when(own)
     def _():
@@ -615,11 +624,8 @@
         for j, out in enumerate((dq, dk, dv)):
             out[...] = (yend[j, 0].astype(F32) + yend[j, 1].astype(F32)).T * 0.125
 
-    for cols in pieces + (beta,):
-        for hf in range(2):
-            net.wait(
-                ("d", cols.start), dbuf.at[hf, :, cols], offset=hf, width=2, when=jnp.logical_or(away, c != hf)
-            )
+    for hf in range(2):
+        net.wait(("d",), dbuf.at[hf], offset=hf, width=2, when=jnp.logical_or(away, c != hf))
 
     @pl.when(own)
     def _():

time: 102 us -> 101 us (level)
  Pallas kernels: 101 us -> 99 us
    pallas_call x1, Pallas kernels: 99.5 us -> 97.9 us  [whole(): pl.pallas_call(whole_kernel, out_shape=(buf(rows, width),) + (buf(depth,...]
where the time goes in v5:
time: 101 us; the launch traced here: 100 us
  Pallas kernels  99 us (98%)
  between operations  1.45 us (1%)
    pallas_call x1, Pallas kernels, whole(): pl.pallas_call(whole_kernel, out_shape=(buf(rows, width),) + (buf(depth,...  97.9 us

profile of v5, /device:TPU:1, one launch (start us, length us, event | category | flops | bytes accessed | tf_op | source)
XLA Modules:
  0.0 100.4 jit_solution(9636330757374193313)
XLA Ops:
  1.3 97.9 %whole.1 = (bf16[128,2048]{1,0:T(8,128)(2,1)S(1)}, f32[256,256]{1,0:T(8,128)S(1)}, f32[256,256]{1,0:T(8,128)S(1)}, f32[256,256]{1,0:T(8,128)S(1)}) custom-call(f32[1]{0:T(128)S(6)} %copy.10.rate, bf16[128,2048]{1,0:T(8,128)(2,1)} %bitcast.4, bf16[128,4096]{1,0:T(8,128)(2,1)} %bitcast.3, bf16[256,256]{1,0:T(8,128)(2,1)} %wq.1, bf16[256,256]{1,0:T(8,128)(2,1)} %wk.1, ...), custom_call_target="tpu_custom_call" | custom-call | tf_op jit(solution)/shard_map/whole/pallas_call | solution.py:653
  99.2 1.1 %finish.1 = (bf16[128,2048]{1,0:T(8,128)(2,1)}, f32[256,256]{1,0:T(8,128)}, f32[256,256]{1,0:T(8,128)}, f32[256,256]{1,0:T(8,128)}) custom-call(bf16[128,2048]{1,0:T(8,128)(2,1)S(1)} %get-tuple-element.12.refs_0_, f32[256,256]{1,0:T(8,128)S(1)} %get-tuple-element.13.refs_1_, f32[256,256]{1,0:T(8,128)S(1)} %get-tuple-element.14.refs_2_, ...), custom_call_target="tpu_custom_call" | custom-call | tf_op jit(solution)/shard_map/finish/pallas_call | solution.py:713

commit v6 on v5

--- a/solution.py
+++ b/solution.py
@@ -10,8 +10,10 @@
 BLOCK = 256
 SIDE = 4
 FIRST = 640
-PIECES = ((512, 128), (0, 256), (256, 256))
+BACK = 512
+PIECES = ((0, 256), (256, 256))
 EAGER = 12
+DEEP = 4
 F32 = jnp.float32
 BF16 = jnp.bfloat16
 MESH = pl.DeviceIdType.MESH
@@ -22,7 +24,7 @@
 GROUP = 4 * 1024 * 1024
 CELL = 32 * 1024
 SENDS = 9
-RECVS = 83
+RECVS = 79
 
 
 def dot(a, b, dims=NN):
@@ -92,7 +94,7 @@
 
 def whole_kernel(
     rate, h_far, c_far, wq, wk, wv, dh, dq, dk, dv,
-    h_all, c_all, w_all, p_all, g_all, g_turn, state, back, rates, inner, inner_t, decays,
+    h_all, c_all, w_all, w_turn, p_all, g_all, g_turn, state, back, rates, inner, inner_t, decays,
     pout, pin, psum, ra1, ra2, ra3, rb0, rb1, rb2, dbuf,
     ysend, yone, yhome, yr1, yr2, yout, yend, h_in, c_in, w_in, local, send, recv,
 ):
@@ -294,6 +296,12 @@
         factor = jnp.where(j == 1, scale, 1.0).astype(F32)
         p_all[place, cols] = (value.astype(F32) * factor).astype(BF16)
 
+    def turn_weight(j):
+        @pl.loop(0, SIDE)
+        def _(t):
+            place = span(t * 2 * depth, 2 * depth, 2 * depth)
+            w_turn[pl.ds(j * columns, columns), place] = w_all[place, pl.ds(j * columns, columns)].T
+
     def project_near(j):
         @pl.loop(0, 3)
         def _(t):
@@ -323,6 +331,7 @@
         mate_wait(r)
     w_ready(0)
     project_near(0)
+    turn_weight(0)
     from_far(0)
     from_far(1)
     for dz, dx in diagonal[EAGER:]:
@@ -338,6 +347,8 @@
     project_near(2)
     fars("a")
     fars("b")
+    turn_weight(1)
+    turn_weight(2)
     mate_wait(2)
     @pl.loop(0, 3)
     def _(j):
@@ -412,14 +423,14 @@
 
     steps = rows * blocks // BLOCK
 
-    @pl.loop(0, steps // 2)
+    @pl.loop(0, steps // DEEP)
     def _(t):
-        for w in range(2):
-            forward(2 * t + w)
-            backward(steps - 1 - 2 * t - w)
+        for w in range(DEEP):
+            forward(DEEP * t + w)
+            backward(steps - 1 - DEEP * t - w)
 
     pieces = tuple(pl.ds(first, size) for first, size in PIECES)
-    beta = pl.ds(FIRST, half - FIRST)
+    beta = pl.ds(BACK, half - BACK)
     chunk = half // 2
 
     def pick_rows(r, hf):
@@ -427,14 +438,14 @@
 
     def other(r, i):
         cols = span(i * chunk, chunk, chunk)
-        value = dot(g_all[r_rows(r), :], w_all[span((1 - c) * half + i * chunk, chunk, chunk), :], NT)
+        value = dot(g_all[r_rows(r), :], w_turn[:, span((1 - c) * half + i * chunk, chunk, chunk)])
         pout[r_rows(r), cols] = value.astype(BF16)
         net.start(("p", r, i), pout.at[r_rows(r), cols], pin.at[r_rows(r), cols], mate)
 
     def summed(r, i):
         cols = span(i * chunk, chunk, chunk)
         net.wait(("p", r, i), pin.at[r_rows(r), cols])
-        value = dot(g_all[r_rows(r), :], w_all[span(c * half + i * chunk, chunk, chunk), :], NT)
+        value = dot(g_all[r_rows(r), :], w_turn[:, span(c * half + i * chunk, chunk, chunk)])
         psum[r_rows(r), cols] = (value + pin[r_rows(r), cols].astype(F32)).astype(BF16)
         if i == 1:
             net.start(("b0", r), psum.at[pick_rows(r, 1 - xl), beta], rb0.at[r % SIDE], pair)
@@ -560,55 +571,49 @@
             net.start(("e", 1), yout.at[j, :, lanes[hf]], yend.at[j, 1], at(xx=cross, cc=hf), when=away)
 
     y_first(0)
+    other(2, 0)
     other(2, 1)
-    other(2, 0)
     y_first(1)
+    summed(2, 0)
+    alpha_first(0)
+    alpha_first(1)
     summed(2, 1)
-    alpha_first(0)
-    summed(2, 0)
-    alpha_first(1)
-    alpha_first(2)
     y_first(2)
+    other(1, 0)
+    other(-1, 0)
     other(1, 1)
     other(-1, 1)
-    other(1, 0)
-    other(-1, 0)
+    summed(1, 0)
+    alpha_plain(0, 1)
+    summed(-1, 0)
+    alpha_plain(0, -1)
     y_second(0)
     summed(1, 1)
-    alpha_plain(0, 1)
     summed(-1, 1)
-    alpha_plain(0, -1)
-    summed(1, 0)
-    alpha_plain(1, 1)
-    summed(-1, 0)
-    alpha_plain(1, -1)
     beta_first()
     alpha_added(0)
+    alpha_plain(1, 1)
+    alpha_plain(1, -1)
     y_second(1)
+    other(0, 0)
     other(0, 1)
-    other(0, 0)
     alpha_added(1)
-    alpha_plain(2, 1)
-    alpha_plain(2, -1)
-    alpha_added(2)
     y_second(2)
-    summed(0, 1)
     summed(0, 0)
     y_home(0)
     y_last(0)
+    alpha_last(0)
+    summed(0, 1)
     y_home(1)
     y_home(2)
+    y_last(1)
     beta_plain()
-    alpha_last(0)
-    y_last(1)
+    beta_added()
     alpha_last(1)
-    beta_added()
     alpha_deliver(0)
-    alpha_last(2)
-    alpha_deliver(1)
     y_last(2)
     beta_last()
-    alpha_deliver(2)
+    alpha_deliver(1)
 
     net.wait(("e", 1), yend.at[:, 1])
     net.wait(("e", 0), yend.at[:, 0], when=away)
@@ -643,7 +648,7 @@
     blocks = SIDE * SIDE
     length = rows * blocks
     half = width // 2
-    rest = half - FIRST
+    rest = half - BACK
     vmem = pl.BlockSpec(memory_space=pltpu.VMEM)
     dma = pltpu.SemaphoreType.DMA
 
@@ -659,6 +664,7 @@
             buf(length, width),
             buf(length, columns),
             buf(depth * 8, 3 * columns),
+            buf(3 * columns, depth * 8),
             buf(length, 3 * columns),
             buf(length, 3 * columns),
             buf(3 * columns, length),
@@ -671,9 +677,9 @@
             buf(length, half),
             buf(length, half),
             buf(length, half),
-            buf(2, 2 * rows, FIRST),
-            buf(2, 4 * rows, FIRST),
-            buf(2 * rows, FIRST),
+            buf(2, 2 * rows, BACK),
+            buf(2, 4 * rows, BACK),
+            buf(2 * rows, BACK),
             buf(SIDE, 2 * rows, rest),
             buf(2, rows, rest),
             buf(2, 2 * rows, rest),

time: 101 us -> 99.4 us (0.984)
  Pallas kernels: 99 us -> 97.8 us
    pallas_call x1, Pallas kernels: 97.9 us -> 96.7 us  [whole(): pl.pallas_call(whole_kernel, out_shape=(buf(rows, width),) + (buf(depth,...]
where the time goes in v6:
time: 99.4 us; the launch traced here: 99.3 us
  Pallas kernels  97.8 us (98%)
  between operations  1.45 us (1%)
    pallas_call x1, Pallas kernels, whole(): pl.pallas_call(whole_kernel, out_shape=(buf(rows, width),) + (buf(depth,...  96.7 us

profile of v6, /device:TPU:1, one launch (start us, length us, event | category | flops | bytes accessed | tf_op | source)
XLA Modules:
  0.0 99.3 jit_solution(12380902543182266464)
XLA Ops:
  1.3 96.7 %whole.1 = (bf16[128,2048]{1,0:T(8,128)(2,1)S(1)}, f32[256,256]{1,0:T(8,128)S(1)}, f32[256,256]{1,0:T(8,128)S(1)}, f32[256,256]{1,0:T(8,128)S(1)}) custom-call(f32[1]{0:T(128)S(6)} %copy.10.rate, bf16[128,2048]{1,0:T(8,128)(2,1)} %bitcast.4, bf16[128,4096]{1,0:T(8,128)(2,1)} %bitcast.3, bf16[256,256]{1,0:T(8,128)(2,1)} %wq.1, bf16[256,256]{1,0:T(8,128)(2,1)} %wk.1, ...), custom_call_target="tpu_custom_call" | custom-call | tf_op jit(solution)/shard_map/whole/pallas_call | solution.py:658
  98.0 1.1 %finish.1 = (bf16[128,2048]{1,0:T(8,128)(2,1)}, f32[256,256]{1,0:T(8,128)}, f32[256,256]{1,0:T(8,128)}, f32[256,256]{1,0:T(8,128)}) custom-call(bf16[128,2048]{1,0:T(8,128)(2,1)S(1)} %get-tuple-element.12.refs_0_, f32[256,256]{1,0:T(8,128)S(1)} %get-tuple-element.13.refs_1_, f32[256,256]{1,0:T(8,128)S(1)} %get-tuple-element.14.refs_2_, ...), custom_call_target="tpu_custom_call" | custom-call | tf_op jit(solution)/shard_map/finish/pallas_call | solution.py:719

commit v7 on v6

--- a/solution.py
+++ b/solution.py
@@ -11,7 +11,8 @@
 SIDE = 4
 FIRST = 640
 BACK = 512
-PIECES = ((0, 256), (256, 256))
+THIN = 128
+PIECES = ((0, 256, 256), (256, 256, 256), (512, THIN, 128))
 EAGER = 12
 DEEP = 4
 F32 = jnp.float32
@@ -24,7 +25,7 @@
 GROUP = 4 * 1024 * 1024
 CELL = 32 * 1024
 SENDS = 9
-RECVS = 79
+RECVS = 88
 
 
 def dot(a, b, dims=NN):
@@ -429,8 +430,10 @@
             forward(DEEP * t + w)
             backward(steps - 1 - DEEP * t - w)
 
-    pieces = tuple(pl.ds(first, size) for first, size in PIECES)
-    beta = pl.ds(BACK, half - BACK)
+    pieces = tuple(pl.ds(first, size) for first, size, _ in PIECES)
+    tall = tuple(size for _, _, size in PIECES)
+    late = (pl.ds(BACK + THIN, half - BACK - THIN), pl.ds(BACK, half - BACK))
+    wide = tuple(pl.ds(0, cols.size) for cols in late)
     chunk = half // 2
 
     def pick_rows(r, hf):
@@ -448,7 +451,8 @@
         value = dot(g_all[r_rows(r), :], w_turn[:, span(c * half + i * chunk, chunk, chunk)])
         psum[r_rows(r), cols] = (value + pin[r_rows(r), cols].astype(F32)).astype(BF16)
         if i == 1:
-            net.start(("b0", r), psum.at[pick_rows(r, 1 - xl), beta], rb0.at[r % SIDE], pair)
+            for b in range(2):
+                net.start(("b0", r, b), psum.at[b_rows(r, b, 1 - xl), late[b]], b0(r, b), pair)
 
     def add(place, cols, *refs):
         total = psum[place, cols].astype(F32)
@@ -456,17 +460,20 @@
             total = total + ref.astype(F32)
         psum[place, cols] = total.astype(BF16)
 
+    def a_rows(i, r, hf):
+        return span(turned(z, r) * four + hf * two, tall[i], tall[i])
+
     def a1(i, e):
-        return ra1.at[e, :, pieces[i]]
+        return ra1.at[e, pl.ds(0, tall[i]), pieces[i]]
 
     def a2(i, e, hf):
-        return ra2.at[e, pl.ds(hf * two, two), pieces[i]]
+        return ra2.at[e, pl.ds(hf * tall[i], tall[i]), pieces[i]]
 
     def a3(i):
-        return ra3.at[:, pieces[i]]
+        return ra3.at[pl.ds(0, tall[i]), pieces[i]]
 
     def alpha_send(i, r, hf, way, name, dst):
-        net.start(name, psum.at[pick_rows(r, hf), pieces[i]], dst, zs[way])
+        net.start(name, psum.at[a_rows(i, r, hf), pieces[i]], dst, zs[way])
 
     def alpha_first(i):
         alpha_send(i, 2, 0, 1, ("a1", i, 0), a1(i, 0))
@@ -479,59 +486,69 @@
     def alpha_added(i):
         for e, r in ((0, 1), (1, -1)):
             net.wait(("a1", i, e), a1(i, e))
-            add(pick_rows(r, e), pieces[i], a1(i, e)[...])
+            add(a_rows(i, r, e), pieces[i], a1(i, e)[...])
             alpha_send(i, r, e, r, ("a2", i), a2(i, e, e))
 
     def alpha_last(i):
-        net.wait(("a2", i), ra2.at[:, :, pieces[i]])
+        net.wait(("a2", i), ra2.at[:, pl.ds(0, 2 * tall[i]), pieces[i]])
         for hf in range(2):
-            add(pick_rows(0, hf), pieces[i], a2(i, 0, hf)[...], a2(i, 1, hf)[...])
-        net.start(("a3", i), psum.at[pick_rows(0, 1 - xl), pieces[i]], a3(i), pair)
-
-    def deliver(cols):
+            add(a_rows(i, 0, hf), pieces[i], a2(i, 0, hf)[...], a2(i, 1, hf)[...])
+        net.start(("a3", i), psum.at[a_rows(i, 0, 1 - xl), pieces[i]], a3(i), pair)
+
+    def deliver(cols, near, far):
         dst = dbuf.at[c, :, cols]
-        net.start(("d",), psum.at[b_rows(0, 1), cols], dst, at(xx=cross, cc=u), offset=c, width=2)
-        net.start(("d",), psum.at[b_rows(0, 0), cols], dst, mate, offset=c, width=2, when=away)
+        if far:
+            net.start(("d",), psum.at[b_rows(0, 1), cols], dst, at(xx=cross, cc=u), offset=c, width=2)
+        if near:
+            net.start(("d",), psum.at[b_rows(0, 0), cols], dst, mate, offset=c, width=2, when=away)
 
     def alpha_deliver(i):
         net.wait(("a3", i), a3(i))
-        add(pick_rows(0, xl), pieces[i], a3(i)[...])
-        deliver(pieces[i])
-
-    def b_rows(r, b):
-        return span(turned(z, r) * four + xl * two + b * rows, rows, rows)
+        add(a_rows(i, 0, xl), pieces[i], a3(i)[...])
+        deliver(pieces[i], True, tall[i] == two)
+
+    def b_rows(r, b, side=xl):
+        return span(turned(z, r) * four + side * two + b * rows, rows, rows)
+
+    def b0(r, b):
+        return rb0.at[r % SIDE, pl.ds(b * rows, rows), wide[b]]
+
+    def b1(b):
+        return rb1.at[b, :, wide[b]]
 
     def b2(e, b):
-        return rb2.at[e, pl.ds(b * rows, rows)]
+        return rb2.at[e, pl.ds(b * rows, rows), wide[b]]
 
     def beta_send(r, b, way, name, dst):
-        net.start(name, psum.at[b_rows(r, b), beta], dst, zs[way])
+        net.start(name, psum.at[b_rows(r, b), late[b]], dst, zs[way])
 
     def beta_take(r):
-        net.wait(("b0", r), rb0.at[r % SIDE])
-        add(pick_rows(r, xl), beta, rb0[r % SIDE])
+        for b in range(2):
+            net.wait(("b0", r, b), b0(r, b))
+            add(b_rows(r, b), late[b], b0(r, b)[...])
 
     def beta_first():
         beta_take(2)
-        beta_send(2, 0, 1, ("b1", 0), rb1.at[0])
-        beta_send(2, 1, -1, ("b1", 1), rb1.at[1])
+        beta_send(2, 0, 1, ("b1", 0), b1(0))
+        beta_send(2, 1, -1, ("b1", 1), b1(1))
 
     def beta_plain():
         for r, b, e in ((1, 1, 0), (-1, 0, 1)):
             beta_take(r)
-            beta_send(r, b, r, ("b2",), b2(e, b))
+            beta_send(r, b, r, ("b2", b), b2(e, b))
 
     def beta_added():
         for r, b, e in ((1, 0, 0), (-1, 1, 1)):
-            net.wait(("b1", e), rb1.at[e])
-            add(b_rows(r, b), beta, rb1[e])
-            beta_send(r, b, r, ("b2",), b2(e, b))
+            net.wait(("b1", e), b1(e))
+            add(b_rows(r, b), late[b], b1(e)[...])
+            beta_send(r, b, r, ("b2", b), b2(e, b))
 
     def beta_last():
         beta_take(0)
-        net.wait(("b2",), rb2)
-        add(pick_rows(0, xl), beta, rb2[0], rb2[1])
-        deliver(beta)
+        for b in (1, 0):
+            net.wait(("b2", b), rb2.at[:, pl.ds(b * rows, rows), wide[b]])
+            add(b_rows(0, b), late[b], b2(0, b)[...], b2(1, b)[...])
+            deliver(late[b], b == 0, b == 1)
 
     lanes = [pl.ds(hf * depth, depth) for hf in range(2)]
 
@@ -578,6 +595,7 @@
     alpha_first(0)
     alpha_first(1)
     summed(2, 1)
+    alpha_first(2)
     y_first(2)
     other(1, 0)
     other(-1, 0)
@@ -594,10 +612,13 @@
     alpha_added(0)
     alpha_plain(1, 1)
     alpha_plain(1, -1)
+    alpha_plain(2, 1)
+    alpha_plain(2, -1)
     y_second(1)
     other(0, 0)
     other(0, 1)
     alpha_added(1)
+    alpha_added(2)
     y_second(2)
     summed(0, 0)
     y_home(0)
@@ -607,10 +628,12 @@
     y_home(1)
     y_home(2)
     y_last(1)
+    alpha_last(2)
     beta_plain()
     beta_added()
     alpha_last(1)
     alpha_deliver(0)
+    alpha_deliver(2)
     y_last(2)
     beta_last()
     alpha_deliver(1)
@@ -677,9 +700,9 @@
             buf(length, half),
             buf(length, half),
             buf(length, half),
-            buf(2, 2 * rows, BACK),
-            buf(2, 4 * rows, BACK),
-            buf(2 * rows, BACK),
+            buf(2, 2 * rows, BACK + THIN),
+            buf(2, 4 * rows, BACK + THIN),
+            buf(2 * rows, BACK + THIN),
             buf(SIDE, 2 * rows, rest),
             buf(2, rows, rest),
             buf(2, 2 * rows, rest),

time: 99.4 us -> 102 us (1.026)
  Pallas kernels: 97.8 us -> 100 us
    pallas_call x1, Pallas kernels: 96.7 us -> 99.1 us  [whole(): pl.pallas_call(whole_kernel, out_shape=(buf(rows, width),) + (buf(depth,...]
where the time goes in v7:
time: 102 us
  Pallas kernels  100 us (98%)
  between operations  1.45 us (1%)
    pallas_call x1, Pallas kernels, whole(): pl.pallas_call(whole_kernel, out_shape=(buf(rows, width),) + (buf(depth,...  99.1 us

profile of v7, /device:TPU:1, one launch (start us, length us, event | category | flops | bytes accessed | tf_op | source)
XLA Modules:
  0.0 101.6 jit_solution(5735020028841726137)
XLA Ops:
  1.3 99.1 %whole.1 = (bf16[128,2048]{1,0:T(8,128)(2,1)S(1)}, f32[256,256]{1,0:T(8,128)S(1)}, f32[256,256]{1,0:T(8,128)S(1)}, f32[256,256]{1,0:T(8,128)S(1)}) custom-call(f32[1]{0:T(128)S(6)} %copy.10.rate, bf16[128,2048]{1,0:T(8,128)(2,1)} %bitcast.4, bf16[128,4096]{1,0:T(8,128)(2,1)} %bitcast.3, bf16[256,256]{1,0:T(8,128)(2,1)} %wq.1, bf16[256,256]{1,0:T(8,128)(2,1)} %wk.1, ...), custom_call_target="tpu_custom_call" | custom-call | tf_op jit(solution)/shard_map/whole/pallas_call | solution.py:681
  100.4 1.1 %finish.1 = (bf16[128,2048]{1,0:T(8,128)(2,1)}, f32[256,256]{1,0:T(8,128)}, f32[256,256]{1,0:T(8,128)}, f32[256,256]{1,0:T(8,128)}) custom-call(bf16[128,2048]{1,0:T(8,128)(2,1)S(1)} %get-tuple-element.12.refs_0_, f32[256,256]{1,0:T(8,128)S(1)} %get-tuple-element.13.refs_1_, f32[256,256]{1,0:T(8,128)S(1)} %get-tuple-element.14.refs_2_, ...), custom_call_target="tpu_custom_call" | custom-call | tf_op jit(solution)/shard_map/finish/pallas_call | solution.py:742

commit v8 on v6

--- a/solution.py
+++ b/solution.py
@@ -9,7 +9,7 @@
 
 BLOCK = 256
 SIDE = 4
-FIRST = 640
+FIRST = 512
 BACK = 512
 PIECES = ((0, 256), (256, 256))
 EAGER = 12

time: 99.4 us -> 99.3 us (level)
  no operation moved by 1% of the time
where the time goes in v8:
time: 99.3 us; the launch traced here: 99.1 us
  Pallas kernels  97.7 us (98%)
  between operations  1.45 us (1%)
    pallas_call x1, Pallas kernels, whole(): pl.pallas_call(whole_kernel, out_shape=(buf(rows, width),) + (buf(depth,...  96.6 us

profile of v8, /device:TPU:1, one launch (start us, length us, event | category | flops | bytes accessed | tf_op | source)
XLA Modules:
  0.0 99.1 jit_solution(1021476797638342968)
XLA Ops:
  1.3 96.6 %whole.1 = (bf16[128,2048]{1,0:T(8,128)(2,1)S(1)}, f32[256,256]{1,0:T(8,128)S(1)}, f32[256,256]{1,0:T(8,128)S(1)}, f32[256,256]{1,0:T(8,128)S(1)}) custom-call(f32[1]{0:T(128)S(6)} %copy.10.rate, bf16[128,2048]{1,0:T(8,128)(2,1)} %bitcast.4, bf16[128,4096]{1,0:T(8,128)(2,1)} %bitcast.3, bf16[256,256]{1,0:T(8,128)(2,1)} %wq.1, bf16[256,256]{1,0:T(8,128)(2,1)} %wk.1, ...), custom_call_target="tpu_custom_call" | custom-call | tf_op jit(solution)/shard_map/whole/pallas_call | solution.py:658
  97.9 1.1 %finish.1 = (bf16[128,2048]{1,0:T(8,128)(2,1)}, f32[256,256]{1,0:T(8,128)}, f32[256,256]{1,0:T(8,128)}, f32[256,256]{1,0:T(8,128)}) custom-call(bf16[128,2048]{1,0:T(8,128)(2,1)S(1)} %get-tuple-element.12.refs_0_, f32[256,256]{1,0:T(8,128)S(1)} %get-tuple-element.13.refs_1_, f32[256,256]{1,0:T(8,128)S(1)} %get-tuple-element.14.refs_2_, ...), custom_call_target="tpu_custom_call" | custom-call | tf_op jit(solution)/shard_map/finish/pallas_call | solution.py:719
